TPU v7x, 256 devices: a 4x2x16 block of a 4x16x16 slice. The times are simulated.
256 devices in a mesh: grp: 2 (over y), sp: 32 (over z, core), tp: 4 (over x).
Axes of the slice: x: 4, y: 2, z: 16, core: 2. Of those that a mesh axis runs over, the one named last changes fastest.
The devices are a block of a 4x16x16 slice.
Arguments:
- query_rows: bfloat16 [8192, 1024], P(('grp', 'sp'), 'tp'), parts along dimension 0, may hold values from -6 to 6
- key_rows: bfloat16 [8192, 1024], P(('grp', 'sp'), 'tp'), parts along dimension 0, may hold values from -6 to 6
- value_rows: bfloat16 [8192, 1024], P(('grp', 'sp'), 'tp'), parts along dimension 0, may hold values from -6 to 6
- gate_rows: bfloat16 [8192, 1024], P(('grp', 'sp'), 'tp'), parts along dimension 0, may hold values from -6 to 6
- log_decay: float32 [2, 8, 8192], P(None, 'tp', ('grp', 'sp')), parts along dimension 2, may hold values from -2 to 0, as said below
- head_gain: float32 [2, 1024], P(None, 'tp'), may hold values from 0.1 to 1.9
- out_weight: bfloat16 [1024, 2048], P('tp'), may hold values from -0.1875 to 0.1875
- residual: bfloat16 [8192, 2048], P(('grp', 'sp')), parts along dimension 0, may hold values from -6 to 6
- norm_gain: bfloat16 [2048], replicated, may hold values from 0.099609375 to 1.8984375
- gate_weight: bfloat16 [2048, 5632], P('sp', 'tp'), may hold values from -0.125 to 0.125
- up_weight: bfloat16 [2048, 5632], P('sp', 'tp'), may hold values from -0.125 to 0.125
- down_weight: bfloat16 [2048, 5632], P('sp', 'tp'), may hold values from -0.078125 to 0.078125
- gate_taps: bfloat16 [3, 5632], P(None, 'tp'), may hold values from -3.5 to 3.5
- up_taps: bfloat16 [3, 5632], P(None, 'tp'), may hold values from -3.5 to 3.5
Outputs:
- block_out: bfloat16 [8192, 2048], P(('grp', 'sp', 'tp')), parts along dimension 0
There are 2 independent parts, one for each index of `grp`. A program takes and returns all parts, laid end to end along the dimension named above; an argument that names none is the same for every part. Nothing has to cross between parts.
Inputs may be any that keep to these rules, and one draw needn't show every extreme that they name: `log_decay`: every entry is negative.
All inputs are finite; a program needn't handle non-finite values.
Results may differ from a plain program's by a relative error of at most 0.017.
Values may be sent and summed in bfloat16 or wider, within the bound.
No kernel may reach another device: no remote copies, remote signals or barrier semaphores. Data moves between devices by JAX's collectives and lax.ppermute only.
A program may use at most 64 MiB of HBM per device.

v0:
```python
import math

import jax
import jax.numpy as jnp
from jax import lax
from jax.experimental import pallas as pl
from jax.experimental.pallas import tpu as pltpu
from jax.sharding import Mesh
from jax.sharding import PartitionSpec as P


HEAD = 128
LANES = 128
SP = ("z", "c")
ROWS = ("pg", "pr", "z", "c")
PEERS = ("pr", "tp")

GROUP_EPS = 1e-05
NORM_EPS = 1e-06


F32 = jnp.float32
BF16 = jnp.bfloat16
VMEM = pl.BlockSpec(memory_space=pltpu.VMEM)
HBM = pl.BlockSpec(memory_space=pltpu.HBM)
BLOCK = 256


def call(body, outs, *args, limit=12, **more):
    spec = {"in_specs": [VMEM] * len(args), "out_specs": jax.tree.map(lambda _: VMEM, outs)}
    return pl.pallas_call(
        body,
        out_shape=outs,
        compiler_params=pltpu.CompilerParams(vmem_limit_bytes=limit << 20),
        **{**spec, **more},
    )(*args)


def shaped(shape, dtype):
    return jax.ShapeDtypeStruct(shape, dtype)


def dot(a, b, dims=((1,), (0,))):
    return lax.dot_general(a, b, (dims, ((), ())), preferred_element_type=F32)


def split_columns(pair, width):
    tiles = width // LANES
    share = -(-tiles // pair)
    step = (tiles - share) // (pair - 1) if pair > 1 else 0
    return share * LANES, step * LANES


def pick_weights(pair, gate_ref, up_ref, down_ref, out_ref, sems):
    cols, step = split_columns(pair, gate_ref.shape[1])
    start = pl.multiple_of(lax.axis_index("pr") * step, LANES)
    blocks = cols // BLOCK
    copies = [
        pltpu.make_async_copy(
            ref.at[:, pl.ds(start + j * BLOCK, BLOCK)],
            out_ref.at[i * blocks + j],
            sems.at[i * blocks + j],
        )
        for i, ref in enumerate((gate_ref, up_ref, down_ref))
        for j in range(blocks)
    ]
    for copy in copies:
        copy.start()
    for copy in copies:
        copy.wait()


def fetch(pairs, sems):
    copies = [pltpu.make_async_copy(src, dst, sems.at[i]) for i, (src, dst) in enumerate(pairs)]
    for copy in copies:
        copy.start()
    return copies


def silu(u):
    return u / (1.0 + jnp.exp(-u))


def local_retention(*refs):
    sources, refs = refs[:6], refs[6:]
    weight_ref, inner_ref, query_ref, gated_ref, keep_ref, send_ref, half_ref, *refs = refs
    held, sems = refs[:6], refs[6]
    half = half_ref.shape[0]
    start = pl.multiple_of(lax.axis_index("c") * half, half)
    copies = fetch(
        [*zip(sources, held), (weight_ref.at[pl.ds(start, half), :], half_ref)], sems
    )
    for copy in copies[:6]:
        copy.wait()
    q_ref, k_ref, v_ref, gate_ref, rate_ref, gain_ref = held
    n, width = q_ref.shape
    heads = width // HEAD
    row = lax.broadcasted_iota(jnp.int32, (n, n), 0)
    col = lax.broadcasted_iota(jnp.int32, (n, n), 1)
    scale = HEAD ** (-0.5)
    first = lax.axis_index("c") == 0
    gated = silu(gate_ref[...].astype(F32))
    for way in range(2):
        gated_ref[way] = gated * gain_ref[way : way + 1, :]
    for h in range(heads):
        cut = slice(h * HEAD, (h + 1) * HEAD)
        q, k, v = q_ref[:, cut], k_ref[:, cut], v_ref[:, cut]
        scores = dot(q, k, ((1,), (1,))) * scale
        states, decays = [], []
        for way in range(2):
            rate = rate_ref[way, h : h + 1, :]
            rate_col = jnp.sum(jnp.where(row == col, rate, 0.0), axis=1, keepdims=True)
            seen = col <= row if way == 0 else col >= row
            seen_by = row <= col if way == 0 else row >= col
            total_col = jnp.sum(jnp.where(seen, rate, 0.0), axis=1, keepdims=True)
            total_row = jnp.sum(jnp.where(seen_by, rate_col, 0.0), axis=0, keepdims=True)
            whole = jnp.sum(rate, axis=1, keepdims=True)
            mask = jnp.where(seen, jnp.exp(jnp.minimum(total_col - total_row, 0.0)), 0.0)
            inner_ref[way, :, cut] = dot((scores * mask).astype(BF16), v)
            query_ref[way, :, cut] = (q.astype(F32) * jnp.exp(total_col)).astype(BF16)
            weight = jnp.exp(whole - total_col) * scale
            states.append(dot((k.astype(F32) * weight).astype(BF16), v, ((0,), (0,))))
            decays.append(jnp.broadcast_to(jnp.exp(whole), (1, HEAD)))
        rows = slice(h * HEAD, (h + 1) * HEAD)
        keep_ref[rows, :] = jnp.where(first, states[0], states[1])
        send_ref[rows, :] = jnp.where(first, states[1], states[0])
        mark = slice(heads * HEAD + h, heads * HEAD + h + 1)
        keep_ref[mark, :] = jnp.where(first, decays[0], decays[1])
        send_ref[mark, :] = jnp.where(first, decays[1], decays[0])
    copies[6].wait()


def pack_states(keep_ref, got_ref, out_ref):
    pieces = out_ref.shape[0]
    heads = keep_ref.shape[0] // HEAD
    rows = HEAD // pieces
    marks = []
    for h in range(heads):
        at = heads * HEAD + h
        a = keep_ref[at : at + 1, :] * got_ref[at : at + 1, :]
        high = a.astype(BF16).astype(F32)
        middle = (a - high).astype(BF16).astype(F32)
        low = a - high - middle
        marks += [high, middle, low]
    used = heads * rows
    marks.append(jnp.zeros((out_ref.shape[1] - used - len(marks), LANES), F32))
    marks = jnp.concatenate(marks, axis=0).astype(BF16)
    for z in range(pieces):
        parts = []
        for h in range(heads):
            at = heads * HEAD + h
            cut = slice(h * HEAD + z * rows, h * HEAD + (z + 1) * rows)
            parts.append(keep_ref[cut, :] * got_ref[at : at + 1, :] + got_ref[cut, :])
        out_ref[z, 0:used, :] = jnp.concatenate(parts, axis=0).astype(BF16)
        out_ref[z, used:, :] = marks


def scan_states(in_ref, out_ref):
    pieces, used, _ = out_ref.shape
    first = lax.axis_index("c") == 0
    half = used // 2
    state = jnp.zeros((used, LANES), F32)
    for t in range(pieces):
        j = jnp.where(first, t, pieces - 1 - t)
        part = in_ref[j].astype(F32)
        out_ref[j] = state.astype(BF16)
        decay = [
            jnp.sum(part[used + 3 * h : used + 3 * h + 3, :], axis=0, keepdims=True)
            for h in range(2)
        ]
        decay = jnp.concatenate([jnp.broadcast_to(d, (half, LANES)) for d in decay], axis=0)
        state = state * decay + part[:used, :]


def spread_states(in_ref, keep_ref, own_ref, send_ref):
    pieces, used, _ = in_ref.shape
    heads = own_ref.shape[0] // HEAD
    rows = used // heads
    for h in range(heads):
        at = heads * HEAD + h
        state = jnp.concatenate(
            [in_ref[z].astype(F32)[h * rows : (h + 1) * rows, :] for z in range(pieces)], axis=0
        )
        cut = slice(h * HEAD, (h + 1) * HEAD)
        own_ref[cut, :] = state.astype(BF16)
        send_ref[cut, :] = (state * keep_ref[at : at + 1, :] + keep_ref[cut, :]).astype(BF16)


def group_norm(values):
    centre = values - jnp.mean(values, axis=1, keepdims=True)
    spread = jnp.mean(centre * centre, axis=1, keepdims=True)
    return centre * lax.rsqrt(spread + GROUP_EPS)


def mix(inner_ref, query_ref, own_ref, got_ref, gated_ref, out_ref):
    heads = inner_ref.shape[2] // HEAD
    first = lax.axis_index("c") == 0
    mixed = []
    for h in range(heads):
        cut = slice(h * HEAD, (h + 1) * HEAD)
        own, got = own_ref[cut, :], got_ref[cut, :]
        combined = 0.0
        for way in range(2):
            state = jnp.where(first, own, got) if way == 0 else jnp.where(first, got, own)
            values = inner_ref[way, :, cut] + dot(query_ref[way, :, cut], state)
            combined = combined + group_norm(values) * gated_ref[way, :, cut]
        mixed.append(combined.astype(BF16))
    mixed = jnp.concatenate(mixed, axis=1)
    for p in range(out_ref.shape[0]):
        out_ref[p] = mixed


def project(pair, tp, *refs):
    mixed_ref, weight_ref, *refs = refs
    near, refs = refs[: tp - 1], refs[tp - 1 :]
    far, refs = refs[: tp - 1], refs[tp - 1 :]
    residuals, refs = refs[:pair], refs[pair:]
    gain_ref, normed_ref, middle_ref, first_ref, last_ref, scratch, table, spans, sems = refs
    me, member, core = lax.axis_index("tp"), lax.axis_index("pr"), lax.axis_index("c")
    n, width = mixed_ref.shape[1:]
    half = width // 2
    low = pl.multiple_of(core * half, half)
    high = pl.multiple_of((1 - core) * half, half)
    pairs = [(weight_ref, table.at[0])]
    for d in range(1, tp):
        pairs.append((near[d - 1], table.at[d, pl.ds(0, half)]))
        pairs.append((far[d - 1], table.at[d, pl.ds(half, half)]))
    pairs += [(residuals[s], spans.at[s]) for s in range(pair)]
    copies = fetch(pairs, sems)
    attended = 0.0
    for d in range(tp):
        parts = []
        for s in range(pair):
            i = lax.rem(member + s, pair) * tp + lax.rem(me - d + tp, tp)
            if d == 0:
                parts.append(mixed_ref[i])
            else:
                parts.append(
                    jnp.concatenate(
                        [mixed_ref[i, :, pl.ds(low, half)], mixed_ref[i, :, pl.ds(high, half)]],
                        axis=1,
                    )
                )
        for copy in copies[max(2 * d - 1, 0) : 2 * d + 1]:
            copy.wait()
        attended = attended + dot(jnp.concatenate(parts, axis=0), table[d])
    for copy in copies[2 * tp - 1 :]:
        copy.wait()
    firsts, lasts = [], []
    for s in range(pair):
        part = attended[s * n : (s + 1) * n, :]
        middle = (spans[s].astype(F32) + part).astype(BF16)
        if s == 0:
            scratch[...] = middle
        values = middle.astype(F32)
        scale = lax.rsqrt(jnp.mean(values * values, axis=1, keepdims=True) + NORM_EPS)
        normed = values * scale * gain_ref[...].astype(F32)
        normed_ref[s * n : (s + 1) * n, :] = normed.astype(BF16)
        firsts.append(normed[0:1, :])
        lasts.append(normed[n - 1 : n, :])
    own = middle_ref.shape[0]
    middle_ref[...] = scratch[pl.ds(pl.multiple_of(me * own, own), own), :]
    fill = [jnp.zeros((first_ref.shape[0] - pair, first_ref.shape[1]), F32)]
    first_ref[...] = jnp.concatenate(firsts + fill, axis=0).astype(BF16)
    last_ref[...] = jnp.concatenate(lasts + fill, axis=0).astype(BF16)


def convolved(pre, pair, taps):
    n = (pre.shape[0] - 16) // pair
    row = lax.broadcasted_iota(jnp.int32, (n, pre.shape[1]), 0)
    spans = []
    for s in range(pair):
        x = pre[s * n : (s + 1) * n, :]
        at = pair * n + s
        before = jnp.where(row == 0, pre[at : at + 1, :], pltpu.roll(x, 1, 0))
        after = jnp.where(row == n - 1, pre[at + 8 : at + 9, :], pltpu.roll(x, n - 1, 0))
        spans.append(taps[0:1] * before + taps[1:2] * x + taps[2:3] * after)
    return jnp.concatenate(spans, axis=0)


def feed_forward(
    pair,
    tp,
    x_ref,
    before_ref,
    after_ref,
    gate_ref,
    up_ref,
    down_ref,
    gt_ref,
    ut_ref,
    out_ref,
    rows_ref,
    acc_ref,
):
    j = pl.program_id(0)
    block = gate_ref.shape[3]
    depth = x_ref.shape[1]
    cols, step = split_columns(pair, gt_ref.shape[1])
    member = lax.axis_index("pr")
    at = pl.multiple_of(member * step + j * block, LANES)
    column = at + lax.broadcasted_iota(jnp.int32, (1, block), 1)
    count = x_ref.shape[0]

    @pl.when(j == 0)
    def _():
        rows_ref[0:count, :] = x_ref[...]
        rows_ref[count:, :] = jnp.concatenate([before_ref[...], after_ref[...]], axis=0)

    def branch(weight, taps):
        pre = dot(rows_ref[...], weight.reshape(depth, block)).astype(BF16).astype(F32)
        return convolved(pre, pair, taps)

    gate = branch(gate_ref[...], gt_ref[:, pl.ds(at, block)].astype(F32))
    taps = jnp.where(column >= member * cols, ut_ref[:, pl.ds(at, block)].astype(F32), 0.0)
    up = branch(up_ref[...], taps)
    hidden = (silu(gate) * up).astype(BF16)
    part = dot(hidden, down_ref[...].reshape(depth, block), ((1,), (1,)))
    last = pl.num_programs(0) - 1

    @pl.when(j == 0)
    def _():
        acc_ref[...] = part

    @pl.when((j > 0) & (j < last))
    def _():
        acc_ref[...] += part

    @pl.when(j == last)
    def _():
        rows = out_ref.shape[1]
        for s in range(pair):
            for q in range(tp):
                cut = slice((s * tp + q) * rows, (s * tp + q + 1) * rows)
                whole = acc_ref[cut, :] + part[cut, :] if cols > block else part[cut, :]
                out_ref[lax.rem(member + s, pair) * tp + q] = whole.astype(BF16)


def run_feed_forward(pair, tp, normed, before, after, gathered, gate_taps, up_taps):
    spans, blocks, height, block = gathered.shape
    depth = spans * height
    steps = blocks // 3
    whole = lambda a: pl.BlockSpec(a.shape, lambda j: (0,) * a.ndim)
    piece = lambda i: pl.BlockSpec(
        (spans, 1, height, block), lambda j, i=i: (0, i * steps + j, 0, 0)
    )
    rows = normed.shape[0]
    out = (pair * tp, rows // (pair * tp), depth)
    return pl.pallas_call(
        lambda *refs: feed_forward(pair, tp, *refs),
        grid=(steps,),
        out_shape=shaped(out, BF16),
        in_specs=[whole(normed), whole(before), whole(after), piece(0), piece(1), piece(2)]
        + [whole(gate_taps), whole(up_taps)],
        out_specs=pl.BlockSpec(out, lambda j: (0, 0, 0)),
        scratch_shapes=[pltpu.VMEM((rows + 16, depth), BF16), pltpu.VMEM((rows, depth), F32)],
        compiler_params=pltpu.CompilerParams(vmem_limit_bytes=56 << 20),
    )(normed, before, after, gathered, gathered, gathered, gate_taps, up_taps)


def across(x, axes):
    return lax.all_to_all(x, axes, 0, 0, tiled=True)


def shards(
    query_rows,
    key_rows,
    value_rows,
    gate_rows,
    log_decay,
    head_gain,
    out_weight,
    residual,
    norm_gain,
    gate_weight,
    up_weight,
    down_weight,
    gate_taps,
    up_taps,
):
    pair, chips, tp = lax.axis_size("pr"), lax.axis_size("z"), lax.axis_size("tp")
    peers = pair * tp
    rows, width = query_rows.shape
    depth = residual.shape[1]
    heads = width // HEAD
    cols, _ = split_columns(pair, gate_weight.shape[1])

    blocks = 3 * cols // BLOCK
    picked = call(
        lambda *refs: pick_weights(pair, *refs),
        shaped((blocks, gate_weight.shape[0], BLOCK), BF16),
        gate_weight,
        up_weight,
        down_weight,
        limit=60,
        in_specs=[HBM] * 3,
        scratch_shapes=[pltpu.SemaphoreType.DMA((blocks,))],
    )
    gathered = lax.all_gather(picked, SP, axis=0, tiled=False)

    marked = shaped((heads * HEAD + 8, HEAD), F32)
    inputs = (query_rows, key_rows, value_rows, gate_rows, log_decay, head_gain)
    inner, query, gated, keep, send, half = call(
        local_retention,
        (
            shaped((2, rows, width), F32),
            shaped((2, rows, width), BF16),
            shaped((2, rows, width), F32),
            marked,
            marked,
            shaped((width // 2, depth), BF16),
        ),
        *inputs,
        out_weight,
        limit=60,
        in_specs=[HBM] * 7,
        scratch_shapes=[pltpu.VMEM(a.shape, a.dtype) for a in inputs]
        + [pltpu.SemaphoreType.DMA((7,))],
    )
    swap = [(0, 1), (1, 0)]
    got = lax.ppermute(send, "c", swap)
    near, far, residuals = [], [], [residual]
    for d in range(1, tp):
        near.append(lax.ppermute(half, "tp", [(i, (i + d) % tp) for i in range(tp)]))
    for a in near:
        far.append(lax.ppermute(a, "c", swap))
    for s in range(1, pair):
        residuals.append(lax.ppermute(residual, "pr", [((i + s) % pair, i) for i in range(pair)]))
    used = heads * HEAD // chips
    message = call(pack_states, shaped((chips, used + 8, HEAD), BF16), keep, got)
    arrived = across(message, "z")
    prefix = call(scan_states, shaped((chips, used, HEAD), BF16), arrived)
    returned = across(prefix, "z")
    state = shaped((heads * HEAD, HEAD), BF16)
    own, other = call(spread_states, (state, state), returned, keep)
    entering = lax.ppermute(other, "c", swap)
    shape = shaped((peers, rows, width), BF16)
    mixed = call(mix, shape, inner, query, own, entering, gated, limit=60)
    edge = shaped((8, depth), BF16)
    normed, middle, first, last = call(
        lambda *refs: project(pair, tp, *refs),
        (shaped((pair * rows, depth), BF16), shaped((rows // tp, depth), BF16), edge, edge),
        across(mixed, PEERS),
        out_weight,
        *near,
        *far,
        *residuals,
        norm_gain.reshape(1, depth),
        limit=60,
        in_specs=[VMEM] + [HBM] * (2 * tp - 1 + pair) + [VMEM],
        scratch_shapes=[
            pltpu.VMEM((rows, depth), BF16),
            pltpu.VMEM((tp, width, depth), BF16),
            pltpu.VMEM((pair, rows, depth), BF16),
            pltpu.SemaphoreType.DMA((2 * tp - 1 + pair,)),
        ],
    )
    size = lax.axis_size("z") * lax.axis_size("c")
    onward = [(i, i + 1) for i in range(size - 1)]
    before = lax.ppermute(last, SP, onward)
    after = lax.ppermute(first, SP, [(j, i) for i, j in onward])
    parts = run_feed_forward(pair, tp, normed, before, after, gathered, gate_taps, up_taps)
    summed = across(parts, PEERS).astype(F32).sum(axis=0)
    return (middle.astype(F32) + summed).astype(BF16)


def solution(mesh):
    groups, tp = mesh.shape["grp"], mesh.shape["tp"]
    pair = math.gcd(groups, 2)
    split = Mesh(
        mesh.devices.reshape(groups // pair, pair, mesh.shape["sp"] // 2, 2, tp),
        ("pg", "pr", "z", "c", "tp"),
    )
    placed = (
        P(ROWS, "tp"),
        P(ROWS, "tp"),
        P(ROWS, "tp"),
        P(ROWS, "tp"),
        P(None, "tp", ROWS),
        P(None, "tp"),
        P("tp", None),
        P(ROWS, None),
        P(),
        P(SP, "tp"),
        P(SP, "tp"),
        P(SP, "tp"),
        P(None, "tp"),
        P(None, "tp"),
    )

    return jax.shard_map(
        shards, mesh=split, in_specs=placed, out_specs=P((*ROWS, "tp"), None), check_vma=False
    )
```

profile of v0, /device:TPU:33, one launch (start us, length us, event | category | flops | bytes accessed | tf_op | source)
XLA Modules:
  0.0 151.3 jit_solution(10513936784735227429)
XLA Ops:
  6.5 0.0 all-gather.3.cloned.1.call-start
  6.6 1.7 %shard_map.142 = bf16[9,64,256]{2,1,0:T(8,128)(2,1)} custom-call(bf16[64,1408]{1,0:T(8,128)(2,1)} %refs_0_.3, bf16[64,1408]{1,0:T(8,128)(2,1)} %refs_1_.5, bf16[64,1408]{1,0:T(8,128)(2,1)} %refs_2_.3), custom_call_target="tpu_custom_call" | custom-call | tf_op jit(solution)/shard_map/pallas_call | solution.py:31
  8.2 0.1 all-gather.3.cloned.1.call-update
  8.3 2.6 %shard_map.136 = (f32[2,128,256]{2,1,0:T(8,128)}, bf16[2,128,256]{2,1,0:T(8,128)(2,1)}, f32[2,128,256]{2,1,0:T(8,128)}, f32[264,128]{1,0:T(8,128)}, f32[264,128]{1,0:T(8,128)}, /*index=5*/bf16[128,2048]{1,0:T(8,128)(2,1)}) custom-call(bf16[128,256]{1,0:T(8,128)(2,1)} %refs_0_.2, bf16[128,256]{1,0:T(8,128)(2,1)} %refs_1_.3, bf16[128,256]{1,0:T(8,128)(2,1)} %refs_2_.2, ...), custom_call_target="tpu_custom_call" | custom-call | tf_op jit(solution)/shard_map/pallas_call | solution.py:31
  11.0 20.5 %collective-permute-start = (f32[264,128]{1,0:T(8,128)}, f32[264,128]{1,0:T(8,128)S(1)}, u32[]{:S(2)}, u32[]{:S(2)}) collective-permute-start(f32[264,128]{1,0:T(8,128)} %get-tuple-element.20), channel_id=1, source_target_pairs={{0,4},{4,0},{1,5},{5,1},{2,6},{6,2},{3,7},{7,3},{8,12},{12,8},{9,1... | collective-permute-start | bytes 405512 | tf_op jit(solution)/shard_map/ppermute | solution.py:421
  31.5 1.2 collective-permute-done.got_ref
  32.7 0.0 copy-start
  32.7 0.9 copy-done
  33.6 16.2 %all_to_all.20.in_ref = bf16[16,24,128]{2,1,0:T(8,128)(2,1)S(1)} all-to-all(bf16[16,24,128]{2,1,0:T(8,128)(2,1)S(1)} %shard_map.137), channel_id=1, replica_groups=mesh['pg'=1,'pr'=2,'z'=16,'c'=2,'tp'=4] {'z'}, dimensions={0} | all-to-all | bytes 196608 | tf_op jit(solution)/shard_map/all_to_all | solution.py:362
  49.9 0.7 shard_map.138
  50.5 6.6 %all-to-all-start.1 = ((bf16[16,16,128]{2,1,0:T(8,128)(2,1)}), bf16[16,16,128]{2,1,0:T(8,128)(2,1)S(1)}, u32[]{:S(2)}, u32[]{:S(2)}) async-start(bf16[16,16,128]{2,1,0:T(8,128)(2,1)} %shard_map.138), calls=%async_computation.1 | async-start | bytes 131072 | tf_op jit(solution)/shard_map/all_to_all | solution.py:362
  57.1 1.5 collective-permute-start.2
  58.6 2.7 %collective-permute-start.3 = (bf16[128,2048]{1,0:T(8,128)(2,1)}, bf16[128,2048]{1,0:T(8,128)(2,1)S(1)}, u32[]{:S(2)}, u32[]{:S(2)}) collective-permute-start(bf16[128,2048]{1,0:T(8,128)(2,1)} %get-tuple-element.24), channel_id=1, source_target_pairs={{0,2},{1,3},{2,0},{3,1},{4,6},{5,7},{6,4},{7,5},{8,10},{9,11},{10,... | collective-permute-start | bytes 1572872 | tf_op jit(solution)/shard_map/ppermute | solution.py:424
  61.3 1.1 collective-permute-start.4
  62.4 6.5 %all-to-all-done.1.in_ref = bf16[16,16,128]{2,1,0:T(8,128)(2,1)S(1)} async-done(((bf16[16,16,128]{2,1,0:T(8,128)(2,1)}), bf16[16,16,128]{2,1,0:T(8,128)(2,1)S(1)}, u32[]{:S(2)}, u32[]{:S(2)}) %all-to-all-start.1) | async-done | bytes 65568 | tf_op jit(solution)/shard_map/all_to_all | solution.py:362
  69.0 0.0 copy-start.1
  69.0 0.9 copy-done.1
  69.9 0.0 copy-start.2
  69.9 0.6 copy-done.2
  70.5 2.5 %collective-permute-start.1 = (bf16[256,128]{1,0:T(8,128)(2,1)S(1)}, bf16[256,128]{1,0:T(8,128)(2,1)S(1)}, u32[]{:S(2)}, u32[]{:S(2)}) collective-permute-start(bf16[256,128]{1,0:T(8,128)(2,1)S(1)} %get-tuple-element.22), channel_id=1, source_target_pairs={{0,4},{4,0},{1,5},{5,1},{2,6},{6,2},{3,7},{7,3},{8,12},{12,8},{9,1... | collective-permute-start | bytes 196616 | tf_op jit(solution)/shard_map/ppermute | solution.py:436
  73.0 0.9 collective-permute-done.1.got_ref
  74.0 0.0 copy-start.11
  74.0 0.6 copy-done.11
  74.6 2.4 %shard_map.140 = bf16[8,128,256]{2,1,0:T(8,128)(2,1)} custom-call(f32[2,128,256]{2,1,0:T(8,128)} %get-tuple-element.17.inner_ref, bf16[2,128,256]{2,1,0:T(8,128)(2,1)} %get-tuple-element.18.query_ref, bf16[256,128]{1,0:T(8,128)(2,1)} %copy-done.2, bf16[256,128]{1,0:T(8,128)(2,1)} %copy-done.11, f32[2,128,256]{2,1,0:T(8,128)} %get-tuple-element.23.gated_ref), custom_call_target="tpu_custom_call" | custom-call | tf_op jit(solution)/shard_map/pallas_call | solution.py:31
  77.0 5.9 %all-to-all-start.2 = ((bf16[8,128,256]{2,1,0:T(8,128)(2,1)}), bf16[8,128,256]{2,1,0:T(8,128)(2,1)S(1)}, u32[]{:S(2)}, u32[]{:S(2)}) async-start(bf16[8,128,256]{2,1,0:T(8,128)(2,1)} %shard_map.140), calls=%async_computation.2 | async-start | bytes 1048576 | tf_op jit(solution)/shard_map/all_to_all | solution.py:362
  82.9 1.5 collective-permute-start.8
  84.3 0.0 collective-permute-done.2.refs_2_
  84.3 0.0 copy-start.4
  84.3 1.2 collective-permute-start.5
  85.5 0.0 collective-permute-done.3.refs_3_
  85.5 0.0 copy-start.5
  85.5 0.1 collective-permute-start.6
  85.7 0.0 collective-permute-done.4.refs_4_
  85.7 0.0 copy-start.6
  85.7 0.4 collective-permute-start.7
  86.0 1.3 reshape.3.refs_10_
  87.3 14.3 %collective-permute-done.8.refs_9_ = bf16[128,2048]{1,0:T(8,128)(2,1)S(1)} collective-permute-done((bf16[128,2048]{1,0:T(8,128)(2,1)}, bf16[128,2048]{1,0:T(8,128)(2,1)S(1)}, u32[]{:S(2)}, u32[]{:S(2)}) %collective-permute-start.8) | collective-permute-done | bytes 524320 | tf_op jit(solution)/shard_map/ppermute | solution.py:428
  101.6 0.0 copy-start.7
  101.6 0.0 collective-permute-done.5.refs_5_
  101.6 0.0 copy-start.8
  101.6 0.0 collective-permute-done.6.refs_6_
  101.6 0.0 copy-start.9
  101.7 0.8 copy-done.9
  102.5 0.0 collective-permute-done.7.refs_7_
  102.5 0.0 all-to-all-done.2.refs_0_
  102.5 0.0 copy-done.4
  102.5 0.0 copy-done.5
  102.5 0.0 copy-done.6
  102.5 0.1 copy-done.7
  102.6 0.2 copy-done.8
  102.8 0.8 copy-done.3
  103.7 5.6 %shard_map.141 = (bf16[256,2048]{1,0:T(8,128)(2,1)}, bf16[32,2048]{1,0:T(8,128)(2,1)}, bf16[8,2048]{1,0:T(8,128)(2,1)}, bf16[8,2048]{1,0:T(8,128)(2,1)}) custom-call(bf16[8,128,256]{2,1,0:T(8,128)(2,1)} %copy-done.3, bf16[256,2048]{1,0:T(8,128)(2,1)} %refs_1_.4, bf16[128,2048]{1,0:T(8,128)(2,1)} %copy-done.4, bf16[128,2048]{1,0:T(8,128)(2,1)} %copy-done.5, ...), custom_call_target="tpu_custom_call" | custom-call | tf_op jit(solution)/shard_map/pallas_call | solution.py:31
  109.2 3.4 %collective-permute-start.10 = (bf16[8,2048]{1,0:T(8,128)(2,1)}, bf16[8,2048]{1,0:T(8,128)(2,1)S(1)}, u32[]{:S(2)}, u32[]{:S(2)}) collective-permute-start(bf16[8,2048]{1,0:T(8,128)(2,1)} %get-tuple-element.28), channel_id=1, source_target_pairs={{4,0},{8,4},{12,8},{16,12},{20,16},{24,20},{28,24},{32,28},{36,32}... | collective-permute-start | bytes 98312 | tf_op jit(solution)/shard_map/ppermute | solution.py:461
  112.6 2.3 %collective-permute-start.9 = (bf16[8,2048]{1,0:T(8,128)(2,1)}, bf16[8,2048]{1,0:T(8,128)(2,1)S(1)}, u32[]{:S(2)}, u32[]{:S(2)}) collective-permute-start(bf16[8,2048]{1,0:T(8,128)(2,1)} %get-tuple-element.27), channel_id=1, source_target_pairs={{0,4},{4,8},{8,12},{12,16},{16,20},{20,24},{24,28},{28,32},{32,36}... | collective-permute-start | bytes 98312 | tf_op jit(solution)/shard_map/ppermute | solution.py:460
  114.9 0.0 collective-permute-done.10.refs_2_
  114.9 0.0 copy-start.12
  114.9 1.3 collective-permute-done.9.refs_1_
  116.2 0.0 copy-done.12
  116.2 0.6 copy-done.13
  116.8 8.2 %shard_map.143 = bf16[8,32,2048]{2,1,0:T(8,128)(2,1)} custom-call(bf16[256,2048]{1,0:T(8,128)(2,1)} %get-tuple-element.26.refs_0_, bf16[8,2048]{1,0:T(8,128)(2,1)} %copy-done.13, bf16[8,2048]{1,0:T(8,128)(2,1)} %copy-done.12, bf16[32,9,64,256]{3,2,1,0:T(8,128)(2,1)} %bitcast.1, bf16[32,9,64,256]{3,2,1,0:T(8,128)(2,1)} %bitcast.2, ...), custom_call_target="tpu_custom_call" | custom-call | tf_op jit(solution)/shard_map/pallas_call | solution.py:349
  125.0 18.6 %all_to_all.21 = bf16[8,32,2048]{2,1,0:T(8,128)(2,1)S(1)} all-to-all(bf16[8,32,2048]{2,1,0:T(8,128)(2,1)} %shard_map.143), channel_id=1, replica_groups=mesh['pg'=1,'pr'=2,'z'=16,'c'=2,'tp'=4] {'pr','tp'}, dimensions={0} | all-to-all | bytes 2097152 | tf_op jit(solution)/shard_map/all_to_all | solution.py:362
  143.6 0.1 convert_reduce_fusion
  143.8 0.0 copy-done.10
  143.8 0.7 add_convert_fusion
  (6 shorter events, 0.1 us)
Async XLA Ops:
  6.5 109.6 %all-gather.3.cloned.1.call-start = ((), (), s32[]{:S(2)}) async-start(), calls=%async_computation.4 | async-start | bytes 9732096 | tf_op jit(solution)/shard_map/all_gather | solution.py:399
  11.0 21.7 %collective-permute-start = (f32[264,128]{1,0:T(8,128)}, f32[264,128]{1,0:T(8,128)S(1)}, u32[]{:S(2)}, u32[]{:S(2)}) collective-permute-start(f32[264,128]{1,0:T(8,128)} %get-tuple-element.20), channel_id=1, source_target_pairs={{0,4},{4,0},{1,5},{5,1},{2,6},{6,2},{3,7},{7,3},{8,12},{12,8},{9,1... | collective-permute-start | bytes 405512 | tf_op jit(solution)/shard_map/ppermute | solution.py:421
  32.7 0.9 copy-start
  50.5 18.4 %all-to-all-start.1 = ((bf16[16,16,128]{2,1,0:T(8,128)(2,1)}), bf16[16,16,128]{2,1,0:T(8,128)(2,1)S(1)}, u32[]{:S(2)}, u32[]{:S(2)}) async-start(bf16[16,16,128]{2,1,0:T(8,128)(2,1)} %shard_map.138), calls=%async_computation.1 | async-start | bytes 131072 | tf_op jit(solution)/shard_map/all_to_all | solution.py:362
  57.1 27.2 %collective-permute-start.2 = (bf16[128,2048]{1,0:T(8,128)(2,1)}, bf16[128,2048]{1,0:T(8,128)(2,1)S(1)}, u32[]{:S(2)}, u32[]{:S(2)}) collective-permute-start(bf16[128,2048]{1,0:T(8,128)(2,1)} %get-tuple-element.24), channel_id=1, source_target_pairs={{0,1},{1,2},{2,3},{3,0},{4,5},{5,6},{6,7},{7,4},{8,9},{9,10},{10,1... | collective-permute-start | bytes 1572872 | tf_op jit(solution)/shard_map/ppermute | solution.py:424
  58.6 26.9 %collective-permute-start.3 = (bf16[128,2048]{1,0:T(8,128)(2,1)}, bf16[128,2048]{1,0:T(8,128)(2,1)S(1)}, u32[]{:S(2)}, u32[]{:S(2)}) collective-permute-start(bf16[128,2048]{1,0:T(8,128)(2,1)} %get-tuple-element.24), channel_id=1, source_target_pairs={{0,2},{1,3},{2,0},{3,1},{4,6},{5,7},{6,4},{7,5},{8,10},{9,11},{10,... | collective-permute-start | bytes 1572872 | tf_op jit(solution)/shard_map/ppermute | solution.py:424
  61.3 24.3 %collective-permute-start.4 = (bf16[128,2048]{1,0:T(8,128)(2,1)}, bf16[128,2048]{1,0:T(8,128)(2,1)S(1)}, u32[]{:S(2)}, u32[]{:S(2)}) collective-permute-start(bf16[128,2048]{1,0:T(8,128)(2,1)} %get-tuple-element.24), channel_id=1, source_target_pairs={{0,3},{1,0},{2,1},{3,2},{4,7},{5,4},{6,5},{7,6},{8,11},{9,8},{10,9... | collective-permute-start | bytes 1572872 | tf_op jit(solution)/shard_map/ppermute | solution.py:424
  69.0 0.9 copy-start.1
  69.9 0.6 copy-start.2
  70.5 3.4 %collective-permute-start.1 = (bf16[256,128]{1,0:T(8,128)(2,1)S(1)}, bf16[256,128]{1,0:T(8,128)(2,1)S(1)}, u32[]{:S(2)}, u32[]{:S(2)}) collective-permute-start(bf16[256,128]{1,0:T(8,128)(2,1)S(1)} %get-tuple-element.22), channel_id=1, source_target_pairs={{0,4},{4,0},{1,5},{5,1},{2,6},{6,2},{3,7},{7,3},{8,12},{12,8},{9,1... | collective-permute-start | bytes 196616 | tf_op jit(solution)/shard_map/ppermute | solution.py:436
  74.0 0.6 copy-start.11
  77.0 25.5 %all-to-all-start.2 = ((bf16[8,128,256]{2,1,0:T(8,128)(2,1)}), bf16[8,128,256]{2,1,0:T(8,128)(2,1)S(1)}, u32[]{:S(2)}, u32[]{:S(2)}) async-start(bf16[8,128,256]{2,1,0:T(8,128)(2,1)} %shard_map.140), calls=%async_computation.2 | async-start | bytes 1048576 | tf_op jit(solution)/shard_map/all_to_all | solution.py:362
  82.9 18.8 %collective-permute-start.8 = (bf16[128,2048]{1,0:T(8,128)(2,1)}, bf16[128,2048]{1,0:T(8,128)(2,1)S(1)}, u32[]{:S(2)}, u32[]{:S(2)}) collective-permute-start(bf16[128,2048]{1,0:T(8,128)(2,1)} %refs_8_.1), channel_id=1, source_target_pairs={{128,0},{0,128},{129,1},{1,129},{130,2},{2,130},{131,3},{3,131},{1... | collective-permute-start | bytes 1572872 | tf_op jit(solution)/shard_map/ppermute | solution.py:428
  84.3 18.2 %copy-start.4 = (bf16[128,2048]{1,0:T(8,128)(2,1)}, bf16[128,2048]{1,0:T(8,128)(2,1)S(1)}, u32[]{:S(2)}) copy-start(bf16[128,2048]{1,0:T(8,128)(2,1)S(1)} %collective-permute-done.2.refs_2_) | copy-start | bytes 1572868
  84.3 17.3 %collective-permute-start.5 = (bf16[128,2048]{1,0:T(8,128)(2,1)S(1)}, bf16[128,2048]{1,0:T(8,128)(2,1)S(1)}, u32[]{:S(2)}, u32[]{:S(2)}) collective-permute-start(bf16[128,2048]{1,0:T(8,128)(2,1)S(1)} %collective-permute-done.2.refs_2_), channel_id=1, source_target_pairs={{0,4},{4,0},{1,5},{5,1},{2,6},{6,2},{3,7},{7,3},{8,12},{12,8},{9,1... | collective-permute-start | bytes 1572872 | tf_op jit(solution)/shard_map/ppermute | solution.py:426
  85.5 17.0 %copy-start.5 = (bf16[128,2048]{1,0:T(8,128)(2,1)}, bf16[128,2048]{1,0:T(8,128)(2,1)S(1)}, u32[]{:S(2)}) copy-start(bf16[128,2048]{1,0:T(8,128)(2,1)S(1)} %collective-permute-done.3.refs_3_) | copy-start | bytes 1572868
  85.5 16.1 %collective-permute-start.6 = (bf16[128,2048]{1,0:T(8,128)(2,1)S(1)}, bf16[128,2048]{1,0:T(8,128)(2,1)S(1)}, u32[]{:S(2)}, u32[]{:S(2)}) collective-permute-start(bf16[128,2048]{1,0:T(8,128)(2,1)S(1)} %collective-permute-done.3.refs_3_), channel_id=1, source_target_pairs={{0,4},{4,0},{1,5},{5,1},{2,6},{6,2},{3,7},{7,3},{8,12},{12,8},{9,1... | collective-permute-start | bytes 1572872 | tf_op jit(solution)/shard_map/ppermute | solution.py:426
  85.7 16.9 %copy-start.6 = (bf16[128,2048]{1,0:T(8,128)(2,1)}, bf16[128,2048]{1,0:T(8,128)(2,1)S(1)}, u32[]{:S(2)}) copy-start(bf16[128,2048]{1,0:T(8,128)(2,1)S(1)} %collective-permute-done.4.refs_4_) | copy-start | bytes 1572868
  85.7 16.8 %collective-permute-start.7 = (bf16[128,2048]{1,0:T(8,128)(2,1)S(1)}, bf16[128,2048]{1,0:T(8,128)(2,1)}, u32[]{:S(2)}, u32[]{:S(2)}) collective-permute-start(bf16[128,2048]{1,0:T(8,128)(2,1)S(1)} %collective-permute-done.4.refs_4_), channel_id=1, source_target_pairs={{0,4},{4,0},{1,5},{5,1},{2,6},{6,2},{3,7},{7,3},{8,12},{12,8},{9,1... | collective-permute-start | bytes 1572872 | tf_op jit(solution)/shard_map/ppermute | solution.py:426
  101.6 1.0 copy-start.7
  101.6 1.2 copy-start.8
  101.6 0.9 copy-start.9
  102.8 0.8 copy-start.3
  109.2 5.7 %collective-permute-start.10 = (bf16[8,2048]{1,0:T(8,128)(2,1)}, bf16[8,2048]{1,0:T(8,128)(2,1)S(1)}, u32[]{:S(2)}, u32[]{:S(2)}) collective-permute-start(bf16[8,2048]{1,0:T(8,128)(2,1)} %get-tuple-element.28), channel_id=1, source_target_pairs={{4,0},{8,4},{12,8},{16,12},{20,16},{24,20},{28,24},{32,28},{36,32}... | collective-permute-start | bytes 98312 | tf_op jit(solution)/shard_map/ppermute | solution.py:461
  112.6 3.6 %collective-permute-start.9 = (bf16[8,2048]{1,0:T(8,128)(2,1)}, bf16[8,2048]{1,0:T(8,128)(2,1)S(1)}, u32[]{:S(2)}, u32[]{:S(2)}) collective-permute-start(bf16[8,2048]{1,0:T(8,128)(2,1)} %get-tuple-element.27), channel_id=1, source_target_pairs={{0,4},{4,8},{8,12},{12,16},{16,20},{20,24},{24,28},{28,32},{32,36}... | collective-permute-start | bytes 98312 | tf_op jit(solution)/shard_map/ppermute | solution.py:460
  114.9 1.3 copy-start.12
  116.2 0.6 copy-start.13
  116.8 27.0 %copy-start.10 = (bf16[32,2048]{1,0:T(8,128)(2,1)S(1)}, bf16[32,2048]{1,0:T(8,128)(2,1)}, u32[]{:S(2)}) copy-start(bf16[32,2048]{1,0:T(8,128)(2,1)} %get-tuple-element.25) | copy-start | bytes 393220
Sparse Core Ops, SparseCore 0:
  9.2 98.9 all-gather.2
where the time goes:
time: 152 us; the launch traced here: 151 us
  starting transfers between devices  49.6 us (33%)
  blocking collectives  34.8 us (23%)
  waiting for transfers between devices  24.3 us (16%)
  Pallas kernels  21.2 us (14%)
  between operations  13.6 us (9%)
  local copies, waits for them, and re-layouts  6.95 us (5%)
    all_to_all x2, blocking collectives, across(): return lax.all_to_all(x, axes, 0, 0, tiled=True)  34.8 us
    ppermute x1, starting transfers between devices, shards(): got = lax.ppermute(send, 'c', swap)  20.5 us
    ppermute x1, waiting for transfers between devices, shards(): lax.ppermute(residual, 'pr', [((i + s) % pair, i) for i in range(pair)])  14.3 us
    pallas_call x7, Pallas kernels, call(): pl.pallas_call(body, out_shape=outs, compiler_params=pltpu.CompilerParams...  13 us
    all_to_all x2, starting transfers between devices, across(): return lax.all_to_all(x, axes, 0, 0, tiled=True)  12.4 us
    pallas_call x1, Pallas kernels, run_feed_forward(): pl.pallas_call(lambda *refs: feed_forward(pair, tp, *refs), grid=(steps,)...  8.23 us
    all_to_all x2, waiting for transfers between devices, across(): return lax.all_to_all(x, axes, 0, 0, tiled=True)  6.55 us
    unnamed x28, local copies, waits for them, and re-layouts  5.66 us
  transfers between devices with their start and end apart: 14, of which 5 were waited for; matrix products, arithmetic and copies ran while one was open for 1% of the time, Pallas kernels for 7%

commit v1 on v0

--- a/solution.py
+++ b/solution.py
@@ -40,6 +40,10 @@
     return jax.ShapeDtypeStruct(shape, dtype)
 
 
+def near_by(shape, dtype):
+    return pltpu.VMEM(shape, dtype)
+
+
 def dot(a, b, dims=((1,), (0,))):
     return lax.dot_general(a, b, (dims, ((), ())), preferred_element_type=F32)
 
@@ -51,23 +55,23 @@
     return share * LANES, step * LANES
 
 
-def pick_weights(pair, gate_ref, up_ref, down_ref, out_ref, sems):
+def pick_weights(pair, gate_ref, up_ref, down_ref, out_ref, held, arrived, left):
     cols, step = split_columns(pair, gate_ref.shape[1])
     start = pl.multiple_of(lax.axis_index("pr") * step, LANES)
     blocks = cols // BLOCK
-    copies = [
-        pltpu.make_async_copy(
-            ref.at[:, pl.ds(start + j * BLOCK, BLOCK)],
-            out_ref.at[i * blocks + j],
-            sems.at[i * blocks + j],
-        )
-        for i, ref in enumerate((gate_ref, up_ref, down_ref))
+    sources = [
+        ref.at[:, pl.ds(start + j * BLOCK, BLOCK)]
+        for ref in (gate_ref, up_ref, down_ref)
         for j in range(blocks)
     ]
-    for copy in copies:
-        copy.start()
-    for copy in copies:
+    copies = fetch([(src, held.at[k]) for k, src in enumerate(sources)], arrived)
+    sends = []
+    for k, copy in enumerate(copies):
         copy.wait()
+        sends.append(pltpu.make_async_copy(held.at[k], out_ref.at[k], left.at[k]))
+        sends[-1].start()
+    for send in sends:
+        send.wait()
 
 
 def fetch(pairs, sems):
@@ -278,84 +282,78 @@
     return jnp.concatenate(spans, axis=0)
 
 
-def feed_forward(
-    pair,
-    tp,
-    x_ref,
-    before_ref,
-    after_ref,
-    gate_ref,
-    up_ref,
-    down_ref,
-    gt_ref,
-    ut_ref,
-    out_ref,
-    rows_ref,
-    acc_ref,
-):
-    j = pl.program_id(0)
-    block = gate_ref.shape[3]
-    depth = x_ref.shape[1]
+def feed_forward(pair, tp, ahead, *refs):
+    x_ref, before_ref, after_ref, table_ref, gt_ref, ut_ref, out_ref, *refs = refs
+    rows_ref, into, back, x_sem, sems = refs
+    _, blocks, _, block = table_ref.shape
+    steps = blocks // 3
+    count, depth = x_ref.shape
+    order = [i * steps + j for j in range(steps) for i in range(2)]
+    order += [2 * steps + j for j in range(steps)]
+    place = lambda i: pl.ds(i * block, block)
+    copies = []
+    for k in order:
+        i, j = k // steps, k % steps
+        target = into.at[j, :, :, place(i)] if i < 2 else back.at[:, :, place(j)]
+        copies.append(pltpu.make_async_copy(table_ref.at[:, k], target, sems.at[k]))
+    rows_copy = pltpu.make_async_copy(x_ref, rows_ref.at[pl.ds(0, count), :], x_sem)
+    rows_copy.start()
+    for copy in copies[:ahead]:
+        copy.start()
+    rows_ref[count:, :] = jnp.concatenate([before_ref[...], after_ref[...]], axis=0)
     cols, step = split_columns(pair, gt_ref.shape[1])
     member = lax.axis_index("pr")
-    at = pl.multiple_of(member * step + j * block, LANES)
-    column = at + lax.broadcasted_iota(jnp.int32, (1, block), 1)
-    count = x_ref.shape[0]
-
-    @pl.when(j == 0)
-    def _():
-        rows_ref[0:count, :] = x_ref[...]
-        rows_ref[count:, :] = jnp.concatenate([before_ref[...], after_ref[...]], axis=0)
-
-    def branch(weight, taps):
-        pre = dot(rows_ref[...], weight.reshape(depth, block)).astype(BF16).astype(F32)
-        return convolved(pre, pair, taps)
-
-    gate = branch(gate_ref[...], gt_ref[:, pl.ds(at, block)].astype(F32))
-    taps = jnp.where(column >= member * cols, ut_ref[:, pl.ds(at, block)].astype(F32), 0.0)
-    up = branch(up_ref[...], taps)
-    hidden = (silu(gate) * up).astype(BF16)
-    part = dot(hidden, down_ref[...].reshape(depth, block), ((1,), (1,)))
-    last = pl.num_programs(0) - 1
-
-    @pl.when(j == 0)
-    def _():
-        acc_ref[...] = part
-
-    @pl.when((j > 0) & (j < last))
-    def _():
-        acc_ref[...] += part
-
-    @pl.when(j == last)
-    def _():
-        rows = out_ref.shape[1]
-        for s in range(pair):
-            for q in range(tp):
-                cut = slice((s * tp + q) * rows, (s * tp + q + 1) * rows)
-                whole = acc_ref[cut, :] + part[cut, :] if cols > block else part[cut, :]
-                out_ref[lax.rem(member + s, pair) * tp + q] = whole.astype(BF16)
-
-
-def run_feed_forward(pair, tp, normed, before, after, gathered, gate_taps, up_taps):
+
+    def arrive(first, last):
+        for i in range(first, last):
+            copies[i].wait()
+            if i + ahead < len(copies):
+                copies[i + ahead].start()
+
+    rows_copy.wait()
+    hidden = []
+    for j in range(steps):
+        at = pl.multiple_of(member * step + j * block, LANES)
+        column = at + lax.broadcasted_iota(jnp.int32, (1, block), 1)
+        up_taps = jnp.where(column >= member * cols, ut_ref[:, pl.ds(at, block)].astype(F32), 0.0)
+        taps = jnp.concatenate([gt_ref[:, pl.ds(at, block)].astype(F32), up_taps], axis=1)
+        arrive(2 * j, 2 * j + 2)
+        pre = dot(rows_ref[...], into[j].reshape(depth, 2 * block)).astype(BF16).astype(F32)
+        both = convolved(pre, pair, taps)
+        hidden.append((silu(both[:, :block]) * both[:, block:]).astype(BF16))
+    arrive(2 * steps, 3 * steps)
+    rows = out_ref.shape[1]
+    whole = back[...].reshape(depth, steps * block)
+    part = dot(jnp.concatenate(hidden, axis=1), whole, ((1,), (1,)))
+    for s in range(pair):
+        for q in range(tp):
+            cut = slice((s * tp + q) * rows, (s * tp + q + 1) * rows)
+            out_ref[lax.rem(member + s, pair) * tp + q] = part[cut, :].astype(BF16)
+
+
+def run_feed_forward(pair, tp, normed, before, after, gathered, gate_taps, up_taps, ahead=6):
     spans, blocks, height, block = gathered.shape
-    depth = spans * height
     steps = blocks // 3
-    whole = lambda a: pl.BlockSpec(a.shape, lambda j: (0,) * a.ndim)
-    piece = lambda i: pl.BlockSpec(
-        (spans, 1, height, block), lambda j, i=i: (0, i * steps + j, 0, 0)
-    )
-    rows = normed.shape[0]
-    out = (pair * tp, rows // (pair * tp), depth)
-    return pl.pallas_call(
-        lambda *refs: feed_forward(pair, tp, *refs),
-        grid=(steps,),
-        out_shape=shaped(out, BF16),
-        in_specs=[whole(normed), whole(before), whole(after), piece(0), piece(1), piece(2)]
-        + [whole(gate_taps), whole(up_taps)],
-        out_specs=pl.BlockSpec(out, lambda j: (0, 0, 0)),
-        scratch_shapes=[pltpu.VMEM((rows + 16, depth), BF16), pltpu.VMEM((rows, depth), F32)],
-        compiler_params=pltpu.CompilerParams(vmem_limit_bytes=56 << 20),
-    )(normed, before, after, gathered, gathered, gathered, gate_taps, up_taps)
+    rows, depth = normed.shape
+    return call(
+        lambda *refs: feed_forward(pair, tp, ahead, *refs),
+        near_by((pair * tp, rows // (pair * tp), depth), BF16),
+        normed,
+        before,
+        after,
+        gathered,
+        gate_taps,
+        up_taps,
+        limit=55,
+        in_specs=[HBM, VMEM, VMEM, HBM, VMEM, VMEM],
+        scratch_shapes=[
+            pltpu.VMEM((rows + 16, depth), BF16),
+            pltpu.VMEM((steps, spans, height, 2 * block), BF16),
+            pltpu.VMEM((spans, height, steps * block), BF16),
+            pltpu.SemaphoreType.DMA,
+            pltpu.SemaphoreType.DMA((blocks,)),
+        ],
+    )
 
 
 def across(x, axes):
@@ -394,18 +392,20 @@
         down_weight,
         limit=60,
         in_specs=[HBM] * 3,
-        scratch_shapes=[pltpu.SemaphoreType.DMA((blocks,))],
+        out_specs=HBM,
+        scratch_shapes=[pltpu.VMEM((blocks, gate_weight.shape[0], BLOCK), BF16)]
+        + [pltpu.SemaphoreType.DMA((blocks,))] * 2,
     )
     gathered = lax.all_gather(picked, SP, axis=0, tiled=False)
 
-    marked = shaped((heads * HEAD + 8, HEAD), F32)
+    marked = near_by((heads * HEAD + 8, HEAD), F32)
     inputs = (query_rows, key_rows, value_rows, gate_rows, log_decay, head_gain)
     inner, query, gated, keep, send, half = call(
         local_retention,
         (
-            shaped((2, rows, width), F32),
-            shaped((2, rows, width), BF16),
-            shaped((2, rows, width), F32),
+            near_by((2, rows, width), F32),
+            near_by((2, rows, width), BF16),
+            near_by((2, rows, width), F32),
             marked,
             marked,
             shaped((width // 2, depth), BF16),
@@ -427,19 +427,19 @@
     for s in range(1, pair):
         residuals.append(lax.ppermute(residual, "pr", [((i + s) % pair, i) for i in range(pair)]))
     used = heads * HEAD // chips
-    message = call(pack_states, shaped((chips, used + 8, HEAD), BF16), keep, got)
+    message = call(pack_states, near_by((chips, used + 8, HEAD), BF16), keep, got)
     arrived = across(message, "z")
-    prefix = call(scan_states, shaped((chips, used, HEAD), BF16), arrived)
+    prefix = call(scan_states, near_by((chips, used, HEAD), BF16), arrived)
     returned = across(prefix, "z")
-    state = shaped((heads * HEAD, HEAD), BF16)
+    state = near_by((heads * HEAD, HEAD), BF16)
     own, other = call(spread_states, (state, state), returned, keep)
     entering = lax.ppermute(other, "c", swap)
-    shape = shaped((peers, rows, width), BF16)
-    mixed = call(mix, shape, inner, query, own, entering, gated, limit=60)
-    edge = shaped((8, depth), BF16)
+    shape = near_by((peers, rows, width), BF16)
+    mixed = call(mix, shape, inner, query, own, entering, gated)
+    edge = near_by((8, depth), BF16)
     normed, middle, first, last = call(
         lambda *refs: project(pair, tp, *refs),
-        (shaped((pair * rows, depth), BF16), shaped((rows // tp, depth), BF16), edge, edge),
+        (near_by((pair * rows, depth), BF16), near_by((rows // tp, depth), BF16), edge, edge),
         across(mixed, PEERS),
         out_weight,
         *near,

time: 152 us -> 145 us (0.954)
  waiting for transfers between devices: 24.3 us -> 18 us
  starting transfers between devices: 49.6 us -> 55.4 us
  Pallas kernels: 21.2 us -> 17.1 us
  local copies, waits for them, and re-layouts: 6.95 us -> 5.35 us
    pallas_call x1 -> x0, Pallas kernels: 8.23 us -> none  [run_feed_forward(): pl.pallas_call(lambda *refs: feed_forward(pair, tp, *refs), grid=(steps,)...]
    ppermute x3, starting transfers between devices: 1.7 us -> 7.2 us  [shards(): far.append(lax.ppermute(a, 'c', swap))]
    ppermute x1, waiting for transfers between devices: 14.3 us -> 8.8 us  [shards(): lax.ppermute(residual, 'pr', [((i + s) % pair, i) for i in range(pair)])]
    pallas_call x7 -> x8, Pallas kernels: 13 us -> 17.1 us  [call(): pl.pallas_call(body, out_shape=outs, compiler_params=pltpu.CompilerParams...]
    unnamed x28 -> x20, local copies, waits for them, and re-layouts: 5.66 us -> 4.06 us
  transfers between devices with their start and end apart: 14 -> 14, of which waited for: 5 -> 5; matrix products, arithmetic and copies ran while one was open for 1% -> 1% of each run, Pallas kernels for 7% -> 6%
where the time goes in v1:
time: 145 us
  starting transfers between devices  55.4 us (38%)
  blocking collectives  34.5 us (24%)
  waiting for transfers between devices  18 us (12%)
  Pallas kernels  17.1 us (12%)
  between operations  13.6 us (9%)
  local copies, waits for them, and re-layouts  5.35 us (4%)
    all_to_all x2, blocking collectives, across(): return lax.all_to_all(x, axes, 0, 0, tiled=True)  34.5 us
    ppermute x1, starting transfers between devices, shards(): got = lax.ppermute(send, 'c', swap)  20.5 us
    pallas_call x8, Pallas kernels, call(): pl.pallas_call(body, out_shape=outs, compiler_params=pltpu.CompilerParams...  17.1 us
    all_to_all x2, starting transfers between devices, across(): return lax.all_to_all(x, axes, 0, 0, tiled=True)  11.6 us
    ppermute x1, waiting for transfers between devices, shards(): lax.ppermute(residual, 'pr', [((i + s) % pair, i) for i in range(pair)])  8.8 us
    ppermute x3, starting transfers between devices, shards(): far.append(lax.ppermute(a, 'c', swap))  7.2 us
    all_to_all x2, waiting for transfers between devices, across(): return lax.all_to_all(x, axes, 0, 0, tiled=True)  6.45 us
    ppermute x3, starting transfers between devices, shards(): lax.ppermute(half, 'tp', [(i, (i + d) % tp) for i in range(tp)])  5.14 us
  transfers between devices with their start and end apart: 14, of which 5 were waited for; matrix products, arithmetic and copies ran while one was open for 1% of the time, Pallas kernels for 6%

profile of v1, /device:TPU:33, one launch (start us, length us, event | category | flops | bytes accessed | tf_op | source)
XLA Modules:
  0.0 144.7 jit_solution(12935969284390328509)
XLA Ops:
  6.5 0.0 all-gather.3.cloned.1.call-start
  6.6 1.7 %shard_map.142 = bf16[9,64,256]{2,1,0:T(8,128)(2,1)} custom-call(bf16[64,1408]{1,0:T(8,128)(2,1)} %refs_0_.3, bf16[64,1408]{1,0:T(8,128)(2,1)} %refs_1_.5, bf16[64,1408]{1,0:T(8,128)(2,1)} %refs_2_.3), custom_call_target="tpu_custom_call" | custom-call | tf_op jit(solution)/shard_map/pallas_call | solution.py:31
  8.2 0.1 all-gather.3.cloned.1.call-update
  8.3 2.3 %shard_map.136 = (f32[2,128,256]{2,1,0:T(8,128)S(1)}, bf16[2,128,256]{2,1,0:T(8,128)(2,1)S(1)}, f32[2,128,256]{2,1,0:T(8,128)S(1)}, f32[264,128]{1,0:T(8,128)S(1...) custom-call(bf16[128,256]{1,0:T(8,128)(2,1)} %refs_0_.2, bf16[128,256]{1,0:T(8,128)(2,1)} %refs_1_.3, ...), custom_call_target="tpu_custom_call" | custom-call | tf_op jit(solution)/shard_map/pallas_call | solution.py:31
  10.6 20.5 %collective-permute-start = (f32[264,128]{1,0:T(8,128)S(1)}, f32[264,128]{1,0:T(8,128)S(1)}, u32[]{:S(2)}, u32[]{:S(2)}) collective-permute-start(f32[264,128]{1,0:T(8,128)S(1)} %get-tuple-element.20), channel_id=1, source_target_pairs={{0,4},{4,0},{1,5},{5,1},{2,6},{6,2},{3,7},{7,3},{8,12},{12,8},{9,1... | collective-permute-start | bytes 405512 | tf_op jit(solution)/shard_map/ppermute | solution.py:421
  31.1 1.0 collective-permute-done.got_ref
  32.2 16.2 %all_to_all.20.in_ref = bf16[16,24,128]{2,1,0:T(8,128)(2,1)S(1)} all-to-all(bf16[16,24,128]{2,1,0:T(8,128)(2,1)S(1)} %shard_map.137), channel_id=1, replica_groups=mesh['pg'=1,'pr'=2,'z'=16,'c'=2,'tp'=4] {'z'}, dimensions={0} | all-to-all | bytes 196608 | tf_op jit(solution)/shard_map/all_to_all | solution.py:360
  48.4 0.7 shard_map.138
  49.1 5.4 %all-to-all-start.1 = ((bf16[16,16,128]{2,1,0:T(8,128)(2,1)}), bf16[16,16,128]{2,1,0:T(8,128)(2,1)S(1)}, u32[]{:S(2)}, u32[]{:S(2)}) async-start(bf16[16,16,128]{2,1,0:T(8,128)(2,1)} %shard_map.138), calls=%async_computation.1 | async-start | bytes 131072 | tf_op jit(solution)/shard_map/all_to_all | solution.py:360
  54.5 1.4 collective-permute-start.2
  55.9 2.8 %collective-permute-start.3 = (bf16[128,2048]{1,0:T(8,128)(2,1)}, bf16[128,2048]{1,0:T(8,128)(2,1)S(1)}, u32[]{:S(2)}, u32[]{:S(2)}) collective-permute-start(bf16[128,2048]{1,0:T(8,128)(2,1)} %get-tuple-element.24), channel_id=1, source_target_pairs={{0,2},{1,3},{2,0},{3,1},{4,6},{5,7},{6,4},{7,5},{8,10},{9,11},{10,... | collective-permute-start | bytes 1572872 | tf_op jit(solution)/shard_map/ppermute | solution.py:424
  58.7 1.0 collective-permute-start.4
  59.6 6.4 %all-to-all-done.1.in_ref = bf16[16,16,128]{2,1,0:T(8,128)(2,1)S(1)} async-done(((bf16[16,16,128]{2,1,0:T(8,128)(2,1)}), bf16[16,16,128]{2,1,0:T(8,128)(2,1)S(1)}, u32[]{:S(2)}, u32[]{:S(2)}) %all-to-all-start.1) | async-done | bytes 65568 | tf_op jit(solution)/shard_map/all_to_all | solution.py:360
  66.1 3.6 %collective-permute-start.1 = (bf16[256,128]{1,0:T(8,128)(2,1)S(1)}, bf16[256,128]{1,0:T(8,128)(2,1)S(1)}, u32[]{:S(2)}, u32[]{:S(2)}) collective-permute-start(bf16[256,128]{1,0:T(8,128)(2,1)S(1)} %get-tuple-element.22), channel_id=1, source_target_pairs={{0,4},{4,0},{1,5},{5,1},{2,6},{6,2},{3,7},{7,3},{8,12},{12,8},{9,1... | collective-permute-start | bytes 196616 | tf_op jit(solution)/shard_map/ppermute | solution.py:436
  69.7 0.9 collective-permute-done.1.got_ref
  70.6 1.2 shard_map.140
  71.8 6.2 %all-to-all-start.2 = ((bf16[8,128,256]{2,1,0:T(8,128)(2,1)}), bf16[8,128,256]{2,1,0:T(8,128)(2,1)S(1)}, u32[]{:S(2)}, u32[]{:S(2)}) async-start(bf16[8,128,256]{2,1,0:T(8,128)(2,1)} %shard_map.140), calls=%async_computation.2 | async-start | bytes 1048576 | tf_op jit(solution)/shard_map/all_to_all | solution.py:360
  78.0 1.5 %collective-permute-start.8 = (bf16[128,2048]{1,0:T(8,128)(2,1)}, bf16[128,2048]{1,0:T(8,128)(2,1)S(1)}, u32[]{:S(2)}, u32[]{:S(2)}) collective-permute-start(bf16[128,2048]{1,0:T(8,128)(2,1)} %refs_8_.1), channel_id=1, source_target_pairs={{128,0},{0,128},{129,1},{1,129},{130,2},{2,130},{131,3},{3,131},{1... | collective-permute-start | bytes 1572872 | tf_op jit(solution)/shard_map/ppermute | solution.py:428
  79.5 0.0 collective-permute-done.2.refs_2_
  79.5 0.0 copy-start.2
  79.5 1.2 collective-permute-start.5
  80.7 0.0 collective-permute-done.3.refs_3_
  80.7 0.0 copy-start.3
  80.7 2.6 %collective-permute-start.6 = (bf16[128,2048]{1,0:T(8,128)(2,1)S(1)}, bf16[128,2048]{1,0:T(8,128)(2,1)S(1)}, u32[]{:S(2)}, u32[]{:S(2)}) collective-permute-start(bf16[128,2048]{1,0:T(8,128)(2,1)S(1)} %collective-permute-done.3.refs_3_), channel_id=1, source_target_pairs={{0,4},{4,0},{1,5},{5,1},{2,6},{6,2},{3,7},{7,3},{8,12},{12,8},{9,1... | collective-permute-start | bytes 1572872 | tf_op jit(solution)/shard_map/ppermute | solution.py:426
  83.3 0.0 collective-permute-done.4.refs_4_
  83.3 0.0 copy-start.4
  83.3 3.4 %collective-permute-start.7 = (bf16[128,2048]{1,0:T(8,128)(2,1)S(1)}, bf16[128,2048]{1,0:T(8,128)(2,1)}, u32[]{:S(2)}, u32[]{:S(2)}) collective-permute-start(bf16[128,2048]{1,0:T(8,128)(2,1)S(1)} %collective-permute-done.4.refs_4_), channel_id=1, source_target_pairs={{0,4},{4,0},{1,5},{5,1},{2,6},{6,2},{3,7},{7,3},{8,12},{12,8},{9,1... | collective-permute-start | bytes 1572872 | tf_op jit(solution)/shard_map/ppermute | solution.py:426
  86.7 1.3 reshape.3.refs_10_
  88.0 8.8 %collective-permute-done.8.refs_9_ = bf16[128,2048]{1,0:T(8,128)(2,1)S(1)} collective-permute-done((bf16[128,2048]{1,0:T(8,128)(2,1)}, bf16[128,2048]{1,0:T(8,128)(2,1)S(1)}, u32[]{:S(2)}, u32[]{:S(2)}) %collective-permute-start.8) | collective-permute-done | bytes 524320 | tf_op jit(solution)/shard_map/ppermute | solution.py:428
  96.8 0.0 copy-start.5
  96.8 0.0 collective-permute-done.5.refs_5_
  96.8 0.0 copy-start.6
  96.8 0.0 collective-permute-done.6.refs_6_
  96.8 0.8 copy-done.6
  97.6 0.0 copy-start.7
  97.6 0.8 copy-done.7
  98.4 0.0 collective-permute-done.7.refs_7_
  98.4 0.0 all-to-all-done.2.refs_0_
  98.4 0.0 copy-done.2
  98.4 0.0 copy-done.3
  98.4 0.0 copy-done.4
  98.5 0.0 copy-done.5
  98.5 0.0 copy-start.1
  98.5 0.8 copy-done.1
  99.3 4.6 %shard_map.141 = (bf16[256,2048]{1,0:T(8,128)(2,1)S(1)}, bf16[32,2048]{1,0:T(8,128)(2,1)S(1)}, bf16[8,2048]{1,0:T(8,128)(2,1)S(1)}, bf16[8,2048]{1,0:T(8,128)(2,1)S(1)}) custom-call(bf16[8,128,256]{2,1,0:T(8,128)(2,1)} %copy-done.1, bf16[256,2048]{1,0:T(8,128)(2,1)} %refs_1_.4, bf16[128,2048]{1,0:T(8,128)(2,1)} %copy-done.2, bf16[128,2048]{1,0:T(8,128)(2,1)} %copy-done.3, ...), custom_call_target="tpu_custom_call" | custom-call | tf_op jit(solution)/shard_map/pallas_call | solution.py:31
  103.8 0.0 copy-start
  103.9 1.0 copy-done
  104.8 3.3 %collective-permute-start.10 = (bf16[8,2048]{1,0:T(8,128)(2,1)S(1)}, bf16[8,2048]{1,0:T(8,128)(2,1)S(1)}, u32[]{:S(2)}, u32[]{:S(2)}) collective-permute-start(bf16[8,2048]{1,0:T(8,128)(2,1)S(1)} %get-tuple-element.28), channel_id=1, source_target_pairs={{4,0},{8,4},{12,8},{16,12},{20,16},{24,20},{28,24},{32,28},{36,32}... | collective-permute-start | bytes 98312 | tf_op jit(solution)/shard_map/ppermute | solution.py:461
  108.2 2.5 %collective-permute-start.9 = (bf16[8,2048]{1,0:T(8,128)(2,1)S(1)}, bf16[8,2048]{1,0:T(8,128)(2,1)S(1)}, u32[]{:S(2)}, u32[]{:S(2)}) collective-permute-start(bf16[8,2048]{1,0:T(8,128)(2,1)S(1)} %get-tuple-element.27), channel_id=1, source_target_pairs={{0,4},{4,8},{8,12},{12,16},{16,20},{20,24},{24,28},{28,32},{32,36}... | collective-permute-start | bytes 98312 | tf_op jit(solution)/shard_map/ppermute | solution.py:460
  110.7 0.0 collective-permute-done.10.refs_2_
  110.7 0.0 copy-start.8
  110.7 0.8 collective-permute-done.9.refs_1_
  111.5 0.0 copy-start.9
  111.5 0.0 all-gather.3.cloned.1.call-done
  111.5 0.0 copy-done.8
  111.5 0.6 copy-done.9
  112.1 6.6 %shard_map.143 = bf16[8,32,2048]{2,1,0:T(8,128)(2,1)S(1)} custom-call(bf16[256,2048]{1,0:T(8,128)(2,1)} %copy-done, bf16[8,2048]{1,0:T(8,128)(2,1)} %copy-done.9, bf16[8,2048]{1,0:T(8,128)(2,1)} %copy-done.8, bf16[32,9,64,256]{3,2,1,0:T(8,128)(2,1)} %bitcast.1, bf16[3,1408]{1,0:T(4,128)(2,1)} %refs_4_.3, bf16[3,1408]{1,0:T(4,128)(2,1)} %refs_5_.3), custom_call_target="tpu_custom_call" | custom-call | tf_op jit(solution)/shard_map/pallas_call | solution.py:31
  118.7 18.2 %all_to_all.21 = bf16[8,32,2048]{2,1,0:T(8,128)(2,1)S(1)} all-to-all(bf16[8,32,2048]{2,1,0:T(8,128)(2,1)S(1)} %shard_map.143), channel_id=1, replica_groups=mesh['pg'=1,'pr'=2,'z'=16,'c'=2,'tp'=4] {'pr','tp'}, dimensions={0} | all-to-all | bytes 2097152 | tf_op jit(solution)/shard_map/all_to_all | solution.py:360
  137.0 0.1 convert_reduce_fusion
  137.1 0.7 add_convert_fusion
  (2 shorter events, 0.0 us)
Async XLA Ops:
  6.5 105.0 %all-gather.3.cloned.1.call-start = ((), (), s32[]{:S(2)}) async-start(), calls=%async_computation.4 | async-start | bytes 9732096 | tf_op jit(solution)/shard_map/all_gather | solution.py:399
  10.6 21.5 %collective-permute-start = (f32[264,128]{1,0:T(8,128)S(1)}, f32[264,128]{1,0:T(8,128)S(1)}, u32[]{:S(2)}, u32[]{:S(2)}) collective-permute-start(f32[264,128]{1,0:T(8,128)S(1)} %get-tuple-element.20), channel_id=1, source_target_pairs={{0,4},{4,0},{1,5},{5,1},{2,6},{6,2},{3,7},{7,3},{8,12},{12,8},{9,1... | collective-permute-start | bytes 405512 | tf_op jit(solution)/shard_map/ppermute | solution.py:421
  49.1 17.0 %all-to-all-start.1 = ((bf16[16,16,128]{2,1,0:T(8,128)(2,1)}), bf16[16,16,128]{2,1,0:T(8,128)(2,1)S(1)}, u32[]{:S(2)}, u32[]{:S(2)}) async-start(bf16[16,16,128]{2,1,0:T(8,128)(2,1)} %shard_map.138), calls=%async_computation.1 | async-start | bytes 131072 | tf_op jit(solution)/shard_map/all_to_all | solution.py:360
  54.5 25.0 %collective-permute-start.2 = (bf16[128,2048]{1,0:T(8,128)(2,1)}, bf16[128,2048]{1,0:T(8,128)(2,1)S(1)}, u32[]{:S(2)}, u32[]{:S(2)}) collective-permute-start(bf16[128,2048]{1,0:T(8,128)(2,1)} %get-tuple-element.24), channel_id=1, source_target_pairs={{0,1},{1,2},{2,3},{3,0},{4,5},{5,6},{6,7},{7,4},{8,9},{9,10},{10,1... | collective-permute-start | bytes 1572872 | tf_op jit(solution)/shard_map/ppermute | solution.py:424
  55.9 24.8 %collective-permute-start.3 = (bf16[128,2048]{1,0:T(8,128)(2,1)}, bf16[128,2048]{1,0:T(8,128)(2,1)S(1)}, u32[]{:S(2)}, u32[]{:S(2)}) collective-permute-start(bf16[128,2048]{1,0:T(8,128)(2,1)} %get-tuple-element.24), channel_id=1, source_target_pairs={{0,2},{1,3},{2,0},{3,1},{4,6},{5,7},{6,4},{7,5},{8,10},{9,11},{10,... | collective-permute-start | bytes 1572872 | tf_op jit(solution)/shard_map/ppermute | solution.py:424
  58.7 24.6 %collective-permute-start.4 = (bf16[128,2048]{1,0:T(8,128)(2,1)}, bf16[128,2048]{1,0:T(8,128)(2,1)S(1)}, u32[]{:S(2)}, u32[]{:S(2)}) collective-permute-start(bf16[128,2048]{1,0:T(8,128)(2,1)} %get-tuple-element.24), channel_id=1, source_target_pairs={{0,3},{1,0},{2,1},{3,2},{4,7},{5,4},{6,5},{7,6},{8,11},{9,8},{10,9... | collective-permute-start | bytes 1572872 | tf_op jit(solution)/shard_map/ppermute | solution.py:424
  66.1 4.5 %collective-permute-start.1 = (bf16[256,128]{1,0:T(8,128)(2,1)S(1)}, bf16[256,128]{1,0:T(8,128)(2,1)S(1)}, u32[]{:S(2)}, u32[]{:S(2)}) collective-permute-start(bf16[256,128]{1,0:T(8,128)(2,1)S(1)} %get-tuple-element.22), channel_id=1, source_target_pairs={{0,4},{4,0},{1,5},{5,1},{2,6},{6,2},{3,7},{7,3},{8,12},{12,8},{9,1... | collective-permute-start | bytes 196616 | tf_op jit(solution)/shard_map/ppermute | solution.py:436
  71.8 26.6 %all-to-all-start.2 = ((bf16[8,128,256]{2,1,0:T(8,128)(2,1)}), bf16[8,128,256]{2,1,0:T(8,128)(2,1)S(1)}, u32[]{:S(2)}, u32[]{:S(2)}) async-start(bf16[8,128,256]{2,1,0:T(8,128)(2,1)} %shard_map.140), calls=%async_computation.2 | async-start | bytes 1048576 | tf_op jit(solution)/shard_map/all_to_all | solution.py:360
  78.0 18.8 %collective-permute-start.8 = (bf16[128,2048]{1,0:T(8,128)(2,1)}, bf16[128,2048]{1,0:T(8,128)(2,1)S(1)}, u32[]{:S(2)}, u32[]{:S(2)}) collective-permute-start(bf16[128,2048]{1,0:T(8,128)(2,1)} %refs_8_.1), channel_id=1, source_target_pairs={{128,0},{0,128},{129,1},{1,129},{130,2},{2,130},{131,3},{3,131},{1... | collective-permute-start | bytes 1572872 | tf_op jit(solution)/shard_map/ppermute | solution.py:428
  79.5 19.0 %copy-start.2 = (bf16[128,2048]{1,0:T(8,128)(2,1)}, bf16[128,2048]{1,0:T(8,128)(2,1)S(1)}, u32[]{:S(2)}) copy-start(bf16[128,2048]{1,0:T(8,128)(2,1)S(1)} %collective-permute-done.2.refs_2_) | copy-start | bytes 1572868
  79.5 17.3 %collective-permute-start.5 = (bf16[128,2048]{1,0:T(8,128)(2,1)S(1)}, bf16[128,2048]{1,0:T(8,128)(2,1)S(1)}, u32[]{:S(2)}, u32[]{:S(2)}) collective-permute-start(bf16[128,2048]{1,0:T(8,128)(2,1)S(1)} %collective-permute-done.2.refs_2_), channel_id=1, source_target_pairs={{0,4},{4,0},{1,5},{5,1},{2,6},{6,2},{3,7},{7,3},{8,12},{12,8},{9,1... | collective-permute-start | bytes 1572872 | tf_op jit(solution)/shard_map/ppermute | solution.py:426
  80.7 17.8 %copy-start.3 = (bf16[128,2048]{1,0:T(8,128)(2,1)}, bf16[128,2048]{1,0:T(8,128)(2,1)S(1)}, u32[]{:S(2)}) copy-start(bf16[128,2048]{1,0:T(8,128)(2,1)S(1)} %collective-permute-done.3.refs_3_) | copy-start | bytes 1572868
  80.7 16.1 %collective-permute-start.6 = (bf16[128,2048]{1,0:T(8,128)(2,1)S(1)}, bf16[128,2048]{1,0:T(8,128)(2,1)S(1)}, u32[]{:S(2)}, u32[]{:S(2)}) collective-permute-start(bf16[128,2048]{1,0:T(8,128)(2,1)S(1)} %collective-permute-done.3.refs_3_), channel_id=1, source_target_pairs={{0,4},{4,0},{1,5},{5,1},{2,6},{6,2},{3,7},{7,3},{8,12},{12,8},{9,1... | collective-permute-start | bytes 1572872 | tf_op jit(solution)/shard_map/ppermute | solution.py:426
  83.3 15.2 %copy-start.4 = (bf16[128,2048]{1,0:T(8,128)(2,1)}, bf16[128,2048]{1,0:T(8,128)(2,1)S(1)}, u32[]{:S(2)}) copy-start(bf16[128,2048]{1,0:T(8,128)(2,1)S(1)} %collective-permute-done.4.refs_4_) | copy-start | bytes 1572868
  83.3 15.2 %collective-permute-start.7 = (bf16[128,2048]{1,0:T(8,128)(2,1)S(1)}, bf16[128,2048]{1,0:T(8,128)(2,1)}, u32[]{:S(2)}, u32[]{:S(2)}) collective-permute-start(bf16[128,2048]{1,0:T(8,128)(2,1)S(1)} %collective-permute-done.4.refs_4_), channel_id=1, source_target_pairs={{0,4},{4,0},{1,5},{5,1},{2,6},{6,2},{3,7},{7,3},{8,12},{12,8},{9,1... | collective-permute-start | bytes 1572872 | tf_op jit(solution)/shard_map/ppermute | solution.py:426
  96.8 1.7 %copy-start.5 = (bf16[128,2048]{1,0:T(8,128)(2,1)}, bf16[128,2048]{1,0:T(8,128)(2,1)S(1)}, u32[]{:S(2)}) copy-start(bf16[128,2048]{1,0:T(8,128)(2,1)S(1)} %collective-permute-done.8.refs_9_) | copy-start | bytes 1572868
  96.8 0.8 copy-start.6
  97.6 0.8 copy-start.7
  98.5 0.8 copy-start.1
  103.8 1.0 copy-start
  104.8 5.8 %collective-permute-start.10 = (bf16[8,2048]{1,0:T(8,128)(2,1)S(1)}, bf16[8,2048]{1,0:T(8,128)(2,1)S(1)}, u32[]{:S(2)}, u32[]{:S(2)}) collective-permute-start(bf16[8,2048]{1,0:T(8,128)(2,1)S(1)} %get-tuple-element.28), channel_id=1, source_target_pairs={{4,0},{8,4},{12,8},{16,12},{20,16},{24,20},{28,24},{32,28},{36,32}... | collective-permute-start | bytes 98312 | tf_op jit(solution)/shard_map/ppermute | solution.py:461
  108.2 3.3 %collective-permute-start.9 = (bf16[8,2048]{1,0:T(8,128)(2,1)S(1)}, bf16[8,2048]{1,0:T(8,128)(2,1)S(1)}, u32[]{:S(2)}, u32[]{:S(2)}) collective-permute-start(bf16[8,2048]{1,0:T(8,128)(2,1)S(1)} %get-tuple-element.27), channel_id=1, source_target_pairs={{0,4},{4,8},{8,12},{12,16},{16,20},{20,24},{24,28},{28,32},{32,36}... | collective-permute-start | bytes 98312 | tf_op jit(solution)/shard_map/ppermute | solution.py:460
  110.7 0.8 copy-start.8
  111.5 0.6 copy-start.9
Sparse Core Ops, SparseCore 0:
  9.2 97.2 all-gather.2

commit v2 on v1

--- a/solution.py
+++ b/solution.py
@@ -283,11 +283,18 @@
 
 
 def feed_forward(pair, tp, ahead, *refs):
-    x_ref, before_ref, after_ref, table_ref, gt_ref, ut_ref, out_ref, *refs = refs
-    rows_ref, into, back, x_sem, sems = refs
+    sources, (table_ref, out_ref), refs = refs[:5], refs[5:7], refs[7:]
+    (before_ref, after_ref, gt_ref, ut_ref, rows_ref, into, back), sems = refs[:7], refs[7:]
     _, blocks, _, block = table_ref.shape
     steps = blocks // 3
-    count, depth = x_ref.shape
+    count, depth = sources[0].shape
+    small = fetch(
+        [
+            *zip(sources[1:], (before_ref, after_ref, gt_ref, ut_ref)),
+            (sources[0], rows_ref.at[pl.ds(0, count), :]),
+        ],
+        sems[0],
+    )
     order = [i * steps + j for j in range(steps) for i in range(2)]
     order += [2 * steps + j for j in range(steps)]
     place = lambda i: pl.ds(i * block, block)
@@ -295,11 +302,11 @@
     for k in order:
         i, j = k // steps, k % steps
         target = into.at[j, :, :, place(i)] if i < 2 else back.at[:, :, place(j)]
-        copies.append(pltpu.make_async_copy(table_ref.at[:, k], target, sems.at[k]))
-    rows_copy = pltpu.make_async_copy(x_ref, rows_ref.at[pl.ds(0, count), :], x_sem)
-    rows_copy.start()
+        copies.append(pltpu.make_async_copy(table_ref.at[:, k], target, sems[1].at[k]))
     for copy in copies[:ahead]:
         copy.start()
+    for copy in small:
+        copy.wait()
     rows_ref[count:, :] = jnp.concatenate([before_ref[...], after_ref[...]], axis=0)
     cols, step = split_columns(pair, gt_ref.shape[1])
     member = lax.axis_index("pr")
@@ -310,7 +317,6 @@
             if i + ahead < len(copies):
                 copies[i + ahead].start()
 
-    rows_copy.wait()
     hidden = []
     for j in range(steps):
         at = pl.multiple_of(member * step + j * block, LANES)
@@ -335,22 +341,20 @@
     spans, blocks, height, block = gathered.shape
     steps = blocks // 3
     rows, depth = normed.shape
+    sources = (normed, before, after, gate_taps, up_taps)
     return call(
         lambda *refs: feed_forward(pair, tp, ahead, *refs),
         near_by((pair * tp, rows // (pair * tp), depth), BF16),
-        normed,
-        before,
-        after,
+        *sources,
         gathered,
-        gate_taps,
-        up_taps,
         limit=55,
-        in_specs=[HBM, VMEM, VMEM, HBM, VMEM, VMEM],
-        scratch_shapes=[
+        in_specs=[HBM] * 6,
+        scratch_shapes=[pltpu.VMEM(a.shape, a.dtype) for a in sources[1:]]
+        + [
             pltpu.VMEM((rows + 16, depth), BF16),
             pltpu.VMEM((steps, spans, height, 2 * block), BF16),
             pltpu.VMEM((spans, height, steps * block), BF16),
-            pltpu.SemaphoreType.DMA,
+            pltpu.SemaphoreType.DMA((5,)),
             pltpu.SemaphoreType.DMA((blocks,)),
         ],
     )

time: 145 us -> 144 us (level)
  no operation moved by 1% of the time
where the time goes in v2:
time: 144 us
  starting transfers between devices  55.4 us (38%)
  blocking collectives  34.5 us (24%)
  waiting for transfers between devices  18 us (12%)
  Pallas kernels  16.4 us (11%)
  between operations  13.6 us (9%)
  local copies, waits for them, and re-layouts  5.35 us (4%)
    all_to_all x2, blocking collectives, across(): return lax.all_to_all(x, axes, 0, 0, tiled=True)  34.5 us
    ppermute x1, starting transfers between devices, shards(): got = lax.ppermute(send, 'c', swap)  20.5 us
    pallas_call x8, Pallas kernels, call(): pl.pallas_call(body, out_shape=outs, compiler_params=pltpu.CompilerParams...  16.4 us
    all_to_all x2, starting transfers between devices, across(): return lax.all_to_all(x, axes, 0, 0, tiled=True)  11.6 us
    ppermute x1, waiting for transfers between devices, shards(): lax.ppermute(residual, 'pr', [((i + s) % pair, i) for i in range(pair)])  8.8 us
    ppermute x3, starting transfers between devices, shards(): far.append(lax.ppermute(a, 'c', swap))  7.2 us
    all_to_all x2, waiting for transfers between devices, across(): return lax.all_to_all(x, axes, 0, 0, tiled=True)  6.45 us
    ppermute x3, starting transfers between devices, shards(): lax.ppermute(half, 'tp', [(i, (i + d) % tp) for i in range(tp)])  5.14 us
  transfers between devices with their start and end apart: 14, of which 5 were waited for; matrix products, arithmetic and copies ran while one was open for 1% of the time, Pallas kernels for 6%

profile of v2, /device:TPU:33, one launch (start us, length us, event | category | flops | bytes accessed | tf_op | source)
XLA Modules:
  0.0 144.0 jit_solution(12071838709763169403)
XLA Ops:
  6.5 0.0 all-gather.3.cloned.1.call-start
  6.6 1.7 %shard_map.142 = bf16[9,64,256]{2,1,0:T(8,128)(2,1)} custom-call(bf16[64,1408]{1,0:T(8,128)(2,1)} %refs_0_.3, bf16[64,1408]{1,0:T(8,128)(2,1)} %refs_1_.5, bf16[64,1408]{1,0:T(8,128)(2,1)} %refs_2_.3), custom_call_target="tpu_custom_call" | custom-call | tf_op jit(solution)/shard_map/pallas_call | solution.py:31
  8.2 0.1 all-gather.3.cloned.1.call-update
  8.3 2.3 %shard_map.136 = (f32[2,128,256]{2,1,0:T(8,128)S(1)}, bf16[2,128,256]{2,1,0:T(8,128)(2,1)S(1)}, f32[2,128,256]{2,1,0:T(8,128)S(1)}, f32[264,128]{1,0:T(8,128)S(1...) custom-call(bf16[128,256]{1,0:T(8,128)(2,1)} %refs_0_.2, bf16[128,256]{1,0:T(8,128)(2,1)} %refs_1_.3, ...), custom_call_target="tpu_custom_call" | custom-call | tf_op jit(solution)/shard_map/pallas_call | solution.py:31
  10.6 20.5 %collective-permute-start = (f32[264,128]{1,0:T(8,128)S(1)}, f32[264,128]{1,0:T(8,128)S(1)}, u32[]{:S(2)}, u32[]{:S(2)}) collective-permute-start(f32[264,128]{1,0:T(8,128)S(1)} %get-tuple-element.20), channel_id=1, source_target_pairs={{0,4},{4,0},{1,5},{5,1},{2,6},{6,2},{3,7},{7,3},{8,12},{12,8},{9,1... | collective-permute-start | bytes 405512 | tf_op jit(solution)/shard_map/ppermute | solution.py:425
  31.1 1.0 collective-permute-done.got_ref
  32.2 16.2 %all_to_all.20.in_ref = bf16[16,24,128]{2,1,0:T(8,128)(2,1)S(1)} all-to-all(bf16[16,24,128]{2,1,0:T(8,128)(2,1)S(1)} %shard_map.137), channel_id=1, replica_groups=mesh['pg'=1,'pr'=2,'z'=16,'c'=2,'tp'=4] {'z'}, dimensions={0} | all-to-all | bytes 196608 | tf_op jit(solution)/shard_map/all_to_all | solution.py:364
  48.4 0.7 shard_map.138
  49.1 5.4 %all-to-all-start.1 = ((bf16[16,16,128]{2,1,0:T(8,128)(2,1)}), bf16[16,16,128]{2,1,0:T(8,128)(2,1)S(1)}, u32[]{:S(2)}, u32[]{:S(2)}) async-start(bf16[16,16,128]{2,1,0:T(8,128)(2,1)} %shard_map.138), calls=%async_computation.1 | async-start | bytes 131072 | tf_op jit(solution)/shard_map/all_to_all | solution.py:364
  54.5 1.4 collective-permute-start.2
  55.9 2.8 %collective-permute-start.3 = (bf16[128,2048]{1,0:T(8,128)(2,1)}, bf16[128,2048]{1,0:T(8,128)(2,1)S(1)}, u32[]{:S(2)}, u32[]{:S(2)}) collective-permute-start(bf16[128,2048]{1,0:T(8,128)(2,1)} %get-tuple-element.24), channel_id=1, source_target_pairs={{0,2},{1,3},{2,0},{3,1},{4,6},{5,7},{6,4},{7,5},{8,10},{9,11},{10,... | collective-permute-start | bytes 1572872 | tf_op jit(solution)/shard_map/ppermute | solution.py:428
  58.7 1.0 collective-permute-start.4
  59.6 6.4 %all-to-all-done.1.in_ref = bf16[16,16,128]{2,1,0:T(8,128)(2,1)S(1)} async-done(((bf16[16,16,128]{2,1,0:T(8,128)(2,1)}), bf16[16,16,128]{2,1,0:T(8,128)(2,1)S(1)}, u32[]{:S(2)}, u32[]{:S(2)}) %all-to-all-start.1) | async-done | bytes 65568 | tf_op jit(solution)/shard_map/all_to_all | solution.py:364
  66.1 3.6 %collective-permute-start.1 = (bf16[256,128]{1,0:T(8,128)(2,1)S(1)}, bf16[256,128]{1,0:T(8,128)(2,1)S(1)}, u32[]{:S(2)}, u32[]{:S(2)}) collective-permute-start(bf16[256,128]{1,0:T(8,128)(2,1)S(1)} %get-tuple-element.22), channel_id=1, source_target_pairs={{0,4},{4,0},{1,5},{5,1},{2,6},{6,2},{3,7},{7,3},{8,12},{12,8},{9,1... | collective-permute-start | bytes 196616 | tf_op jit(solution)/shard_map/ppermute | solution.py:440
  69.7 0.9 collective-permute-done.1.got_ref
  70.6 1.2 shard_map.140
  71.8 6.2 %all-to-all-start.2 = ((bf16[8,128,256]{2,1,0:T(8,128)(2,1)}), bf16[8,128,256]{2,1,0:T(8,128)(2,1)S(1)}, u32[]{:S(2)}, u32[]{:S(2)}) async-start(bf16[8,128,256]{2,1,0:T(8,128)(2,1)} %shard_map.140), calls=%async_computation.2 | async-start | bytes 1048576 | tf_op jit(solution)/shard_map/all_to_all | solution.py:364
  78.0 1.5 %collective-permute-start.8 = (bf16[128,2048]{1,0:T(8,128)(2,1)}, bf16[128,2048]{1,0:T(8,128)(2,1)S(1)}, u32[]{:S(2)}, u32[]{:S(2)}) collective-permute-start(bf16[128,2048]{1,0:T(8,128)(2,1)} %refs_8_.1), channel_id=1, source_target_pairs={{128,0},{0,128},{129,1},{1,129},{130,2},{2,130},{131,3},{3,131},{1... | collective-permute-start | bytes 1572872 | tf_op jit(solution)/shard_map/ppermute | solution.py:432
  79.5 0.0 collective-permute-done.2.refs_2_
  79.5 0.0 copy-start.2
  79.5 1.2 collective-permute-start.5
  80.7 0.0 collective-permute-done.3.refs_3_
  80.7 0.0 copy-start.3
  80.7 2.6 %collective-permute-start.6 = (bf16[128,2048]{1,0:T(8,128)(2,1)S(1)}, bf16[128,2048]{1,0:T(8,128)(2,1)S(1)}, u32[]{:S(2)}, u32[]{:S(2)}) collective-permute-start(bf16[128,2048]{1,0:T(8,128)(2,1)S(1)} %collective-permute-done.3.refs_3_), channel_id=1, source_target_pairs={{0,4},{4,0},{1,5},{5,1},{2,6},{6,2},{3,7},{7,3},{8,12},{12,8},{9,1... | collective-permute-start | bytes 1572872 | tf_op jit(solution)/shard_map/ppermute | solution.py:430
  83.3 0.0 collective-permute-done.4.refs_4_
  83.3 0.0 copy-start.4
  83.3 3.4 %collective-permute-start.7 = (bf16[128,2048]{1,0:T(8,128)(2,1)S(1)}, bf16[128,2048]{1,0:T(8,128)(2,1)}, u32[]{:S(2)}, u32[]{:S(2)}) collective-permute-start(bf16[128,2048]{1,0:T(8,128)(2,1)S(1)} %collective-permute-done.4.refs_4_), channel_id=1, source_target_pairs={{0,4},{4,0},{1,5},{5,1},{2,6},{6,2},{3,7},{7,3},{8,12},{12,8},{9,1... | collective-permute-start | bytes 1572872 | tf_op jit(solution)/shard_map/ppermute | solution.py:430
  86.7 1.3 reshape.3.refs_10_
  88.0 8.8 %collective-permute-done.8.refs_9_ = bf16[128,2048]{1,0:T(8,128)(2,1)S(1)} collective-permute-done((bf16[128,2048]{1,0:T(8,128)(2,1)}, bf16[128,2048]{1,0:T(8,128)(2,1)S(1)}, u32[]{:S(2)}, u32[]{:S(2)}) %collective-permute-start.8) | collective-permute-done | bytes 524320 | tf_op jit(solution)/shard_map/ppermute | solution.py:432
  96.8 0.0 copy-start.5
  96.8 0.0 collective-permute-done.5.refs_5_
  96.8 0.0 copy-start.6
  96.8 0.0 collective-permute-done.6.refs_6_
  96.8 0.8 copy-done.6
  97.6 0.0 copy-start.7
  97.6 0.8 copy-done.7
  98.4 0.0 collective-permute-done.7.refs_7_
  98.4 0.0 all-to-all-done.2.refs_0_
  98.4 0.0 copy-done.2
  98.4 0.0 copy-done.3
  98.4 0.0 copy-done.4
  98.5 0.0 copy-done.5
  98.5 0.0 copy-start.1
  98.5 0.8 copy-done.1
  99.3 4.6 %shard_map.141 = (bf16[256,2048]{1,0:T(8,128)(2,1)S(1)}, bf16[32,2048]{1,0:T(8,128)(2,1)S(1)}, bf16[8,2048]{1,0:T(8,128)(2,1)S(1)}, bf16[8,2048]{1,0:T(8,128)(2,1)S(1)}) custom-call(bf16[8,128,256]{2,1,0:T(8,128)(2,1)} %copy-done.1, bf16[256,2048]{1,0:T(8,128)(2,1)} %refs_1_.4, bf16[128,2048]{1,0:T(8,128)(2,1)} %copy-done.2, bf16[128,2048]{1,0:T(8,128)(2,1)} %copy-done.3, ...), custom_call_target="tpu_custom_call" | custom-call | tf_op jit(solution)/shard_map/pallas_call | solution.py:31
  103.8 0.0 copy-start
  103.9 1.0 copy-done
  104.8 3.3 %collective-permute-start.10 = (bf16[8,2048]{1,0:T(8,128)(2,1)S(1)}, bf16[8,2048]{1,0:T(8,128)(2,1)S(1)}, u32[]{:S(2)}, u32[]{:S(2)}) collective-permute-start(bf16[8,2048]{1,0:T(8,128)(2,1)S(1)} %get-tuple-element.28), channel_id=1, source_target_pairs={{4,0},{8,4},{12,8},{16,12},{20,16},{24,20},{28,24},{32,28},{36,32}... | collective-permute-start | bytes 98312 | tf_op jit(solution)/shard_map/ppermute | solution.py:465
  108.2 2.5 %collective-permute-start.9 = (bf16[8,2048]{1,0:T(8,128)(2,1)S(1)}, bf16[8,2048]{1,0:T(8,128)(2,1)S(1)}, u32[]{:S(2)}, u32[]{:S(2)}) collective-permute-start(bf16[8,2048]{1,0:T(8,128)(2,1)S(1)} %get-tuple-element.27), channel_id=1, source_target_pairs={{0,4},{4,8},{8,12},{12,16},{16,20},{20,24},{24,28},{28,32},{32,36}... | collective-permute-start | bytes 98312 | tf_op jit(solution)/shard_map/ppermute | solution.py:464
  110.7 0.0 collective-permute-done.10.refs_2_
  110.7 0.0 copy-start.8
  110.7 0.8 collective-permute-done.9.refs_1_
  111.5 0.0 copy-start.9
  111.5 0.0 all-gather.3.cloned.1.call-done
  111.5 0.0 copy-done.8
  111.5 0.6 copy-done.9
  112.1 5.9 %shard_map.143 = bf16[8,32,2048]{2,1,0:T(8,128)(2,1)S(1)} custom-call(bf16[256,2048]{1,0:T(8,128)(2,1)} %copy-done, bf16[8,2048]{1,0:T(8,128)(2,1)} %copy-done.9, bf16[8,2048]{1,0:T(8,128)(2,1)} %copy-done.8, bf16[3,1408]{1,0:T(4,128)(2,1)} %refs_3_.3, bf16[3,1408]{1,0:T(4,128)(2,1)} %refs_4_.3, bf16[32,9,64,256]{3,2,1,0:T(8,128)(2,1)} %bitcast.1), custom_call_target="tpu_custom_call" | custom-call | tf_op jit(solution)/shard_map/pallas_call | solution.py:31
  118.0 18.2 %all_to_all.21 = bf16[8,32,2048]{2,1,0:T(8,128)(2,1)S(1)} all-to-all(bf16[8,32,2048]{2,1,0:T(8,128)(2,1)S(1)} %shard_map.143), channel_id=1, replica_groups=mesh['pg'=1,'pr'=2,'z'=16,'c'=2,'tp'=4] {'pr','tp'}, dimensions={0} | all-to-all | bytes 2097152 | tf_op jit(solution)/shard_map/all_to_all | solution.py:364
  136.3 0.1 convert_reduce_fusion
  136.4 0.7 add_convert_fusion
  (2 shorter events, 0.0 us)
Async XLA Ops:
  6.5 105.0 %all-gather.3.cloned.1.call-start = ((), (), s32[]{:S(2)}) async-start(), calls=%async_computation.4 | async-start | bytes 9732096 | tf_op jit(solution)/shard_map/all_gather | solution.py:403
  10.6 21.5 %collective-permute-start = (f32[264,128]{1,0:T(8,128)S(1)}, f32[264,128]{1,0:T(8,128)S(1)}, u32[]{:S(2)}, u32[]{:S(2)}) collective-permute-start(f32[264,128]{1,0:T(8,128)S(1)} %get-tuple-element.20), channel_id=1, source_target_pairs={{0,4},{4,0},{1,5},{5,1},{2,6},{6,2},{3,7},{7,3},{8,12},{12,8},{9,1... | collective-permute-start | bytes 405512 | tf_op jit(solution)/shard_map/ppermute | solution.py:425
  49.1 17.0 %all-to-all-start.1 = ((bf16[16,16,128]{2,1,0:T(8,128)(2,1)}), bf16[16,16,128]{2,1,0:T(8,128)(2,1)S(1)}, u32[]{:S(2)}, u32[]{:S(2)}) async-start(bf16[16,16,128]{2,1,0:T(8,128)(2,1)} %shard_map.138), calls=%async_computation.1 | async-start | bytes 131072 | tf_op jit(solution)/shard_map/all_to_all | solution.py:364
  54.5 25.0 %collective-permute-start.2 = (bf16[128,2048]{1,0:T(8,128)(2,1)}, bf16[128,2048]{1,0:T(8,128)(2,1)S(1)}, u32[]{:S(2)}, u32[]{:S(2)}) collective-permute-start(bf16[128,2048]{1,0:T(8,128)(2,1)} %get-tuple-element.24), channel_id=1, source_target_pairs={{0,1},{1,2},{2,3},{3,0},{4,5},{5,6},{6,7},{7,4},{8,9},{9,10},{10,1... | collective-permute-start | bytes 1572872 | tf_op jit(solution)/shard_map/ppermute | solution.py:428
  55.9 24.8 %collective-permute-start.3 = (bf16[128,2048]{1,0:T(8,128)(2,1)}, bf16[128,2048]{1,0:T(8,128)(2,1)S(1)}, u32[]{:S(2)}, u32[]{:S(2)}) collective-permute-start(bf16[128,2048]{1,0:T(8,128)(2,1)} %get-tuple-element.24), channel_id=1, source_target_pairs={{0,2},{1,3},{2,0},{3,1},{4,6},{5,7},{6,4},{7,5},{8,10},{9,11},{10,... | collective-permute-start | bytes 1572872 | tf_op jit(solution)/shard_map/ppermute | solution.py:428
  58.7 24.6 %collective-permute-start.4 = (bf16[128,2048]{1,0:T(8,128)(2,1)}, bf16[128,2048]{1,0:T(8,128)(2,1)S(1)}, u32[]{:S(2)}, u32[]{:S(2)}) collective-permute-start(bf16[128,2048]{1,0:T(8,128)(2,1)} %get-tuple-element.24), channel_id=1, source_target_pairs={{0,3},{1,0},{2,1},{3,2},{4,7},{5,4},{6,5},{7,6},{8,11},{9,8},{10,9... | collective-permute-start | bytes 1572872 | tf_op jit(solution)/shard_map/ppermute | solution.py:428
  66.1 4.5 %collective-permute-start.1 = (bf16[256,128]{1,0:T(8,128)(2,1)S(1)}, bf16[256,128]{1,0:T(8,128)(2,1)S(1)}, u32[]{:S(2)}, u32[]{:S(2)}) collective-permute-start(bf16[256,128]{1,0:T(8,128)(2,1)S(1)} %get-tuple-element.22), channel_id=1, source_target_pairs={{0,4},{4,0},{1,5},{5,1},{2,6},{6,2},{3,7},{7,3},{8,12},{12,8},{9,1... | collective-permute-start | bytes 196616 | tf_op jit(solution)/shard_map/ppermute | solution.py:440
  71.8 26.6 %all-to-all-start.2 = ((bf16[8,128,256]{2,1,0:T(8,128)(2,1)}), bf16[8,128,256]{2,1,0:T(8,128)(2,1)S(1)}, u32[]{:S(2)}, u32[]{:S(2)}) async-start(bf16[8,128,256]{2,1,0:T(8,128)(2,1)} %shard_map.140), calls=%async_computation.2 | async-start | bytes 1048576 | tf_op jit(solution)/shard_map/all_to_all | solution.py:364
  78.0 18.8 %collective-permute-start.8 = (bf16[128,2048]{1,0:T(8,128)(2,1)}, bf16[128,2048]{1,0:T(8,128)(2,1)S(1)}, u32[]{:S(2)}, u32[]{:S(2)}) collective-permute-start(bf16[128,2048]{1,0:T(8,128)(2,1)} %refs_8_.1), channel_id=1, source_target_pairs={{128,0},{0,128},{129,1},{1,129},{130,2},{2,130},{131,3},{3,131},{1... | collective-permute-start | bytes 1572872 | tf_op jit(solution)/shard_map/ppermute | solution.py:432
  79.5 19.0 %copy-start.2 = (bf16[128,2048]{1,0:T(8,128)(2,1)}, bf16[128,2048]{1,0:T(8,128)(2,1)S(1)}, u32[]{:S(2)}) copy-start(bf16[128,2048]{1,0:T(8,128)(2,1)S(1)} %collective-permute-done.2.refs_2_) | copy-start | bytes 1572868
  79.5 17.3 %collective-permute-start.5 = (bf16[128,2048]{1,0:T(8,128)(2,1)S(1)}, bf16[128,2048]{1,0:T(8,128)(2,1)S(1)}, u32[]{:S(2)}, u32[]{:S(2)}) collective-permute-start(bf16[128,2048]{1,0:T(8,128)(2,1)S(1)} %collective-permute-done.2.refs_2_), channel_id=1, source_target_pairs={{0,4},{4,0},{1,5},{5,1},{2,6},{6,2},{3,7},{7,3},{8,12},{12,8},{9,1... | collective-permute-start | bytes 1572872 | tf_op jit(solution)/shard_map/ppermute | solution.py:430
  80.7 17.8 %copy-start.3 = (bf16[128,2048]{1,0:T(8,128)(2,1)}, bf16[128,2048]{1,0:T(8,128)(2,1)S(1)}, u32[]{:S(2)}) copy-start(bf16[128,2048]{1,0:T(8,128)(2,1)S(1)} %collective-permute-done.3.refs_3_) | copy-start | bytes 1572868
  80.7 16.1 %collective-permute-start.6 = (bf16[128,2048]{1,0:T(8,128)(2,1)S(1)}, bf16[128,2048]{1,0:T(8,128)(2,1)S(1)}, u32[]{:S(2)}, u32[]{:S(2)}) collective-permute-start(bf16[128,2048]{1,0:T(8,128)(2,1)S(1)} %collective-permute-done.3.refs_3_), channel_id=1, source_target_pairs={{0,4},{4,0},{1,5},{5,1},{2,6},{6,2},{3,7},{7,3},{8,12},{12,8},{9,1... | collective-permute-start | bytes 1572872 | tf_op jit(solution)/shard_map/ppermute | solution.py:430
  83.3 15.2 %copy-start.4 = (bf16[128,2048]{1,0:T(8,128)(2,1)}, bf16[128,2048]{1,0:T(8,128)(2,1)S(1)}, u32[]{:S(2)}) copy-start(bf16[128,2048]{1,0:T(8,128)(2,1)S(1)} %collective-permute-done.4.refs_4_) | copy-start | bytes 1572868
  83.3 15.2 %collective-permute-start.7 = (bf16[128,2048]{1,0:T(8,128)(2,1)S(1)}, bf16[128,2048]{1,0:T(8,128)(2,1)}, u32[]{:S(2)}, u32[]{:S(2)}) collective-permute-start(bf16[128,2048]{1,0:T(8,128)(2,1)S(1)} %collective-permute-done.4.refs_4_), channel_id=1, source_target_pairs={{0,4},{4,0},{1,5},{5,1},{2,6},{6,2},{3,7},{7,3},{8,12},{12,8},{9,1... | collective-permute-start | bytes 1572872 | tf_op jit(solution)/shard_map/ppermute | solution.py:430
  96.8 1.7 %copy-start.5 = (bf16[128,2048]{1,0:T(8,128)(2,1)}, bf16[128,2048]{1,0:T(8,128)(2,1)S(1)}, u32[]{:S(2)}) copy-start(bf16[128,2048]{1,0:T(8,128)(2,1)S(1)} %collective-permute-done.8.refs_9_) | copy-start | bytes 1572868
  96.8 0.8 copy-start.6
  97.6 0.8 copy-start.7
  98.5 0.8 copy-start.1
  103.8 1.0 copy-start
  104.8 5.8 %collective-permute-start.10 = (bf16[8,2048]{1,0:T(8,128)(2,1)S(1)}, bf16[8,2048]{1,0:T(8,128)(2,1)S(1)}, u32[]{:S(2)}, u32[]{:S(2)}) collective-permute-start(bf16[8,2048]{1,0:T(8,128)(2,1)S(1)} %get-tuple-element.28), channel_id=1, source_target_pairs={{4,0},{8,4},{12,8},{16,12},{20,16},{24,20},{28,24},{32,28},{36,32}... | collective-permute-start | bytes 98312 | tf_op jit(solution)/shard_map/ppermute | solution.py:465
  108.2 3.3 %collective-permute-start.9 = (bf16[8,2048]{1,0:T(8,128)(2,1)S(1)}, bf16[8,2048]{1,0:T(8,128)(2,1)S(1)}, u32[]{:S(2)}, u32[]{:S(2)}) collective-permute-start(bf16[8,2048]{1,0:T(8,128)(2,1)S(1)} %get-tuple-element.27), channel_id=1, source_target_pairs={{0,4},{4,8},{8,12},{12,16},{16,20},{20,24},{24,28},{28,32},{32,36}... | collective-permute-start | bytes 98312 | tf_op jit(solution)/shard_map/ppermute | solution.py:464
  110.7 0.8 copy-start.8
  111.5 0.6 copy-start.9
Sparse Core Ops, SparseCore 0:
  9.2 97.2 all-gather.2
